TPU v7x, 32 devices: a whole 2x2x4 slice. The times are simulated.
32 devices in a mesh: sp: 16 (over z, y, x), tp: 2 (over core).
Axes of the slice: x: 2, y: 2, z: 4, core: 2. Of those that a mesh axis runs over, the one named last changes fastest.
Arguments:
- tokens: bfloat16 [3072, 4096], P('sp'), may hold values from -6 to 6
- norm_gain: float32 [4096], replicated, may hold values from 0.1 to 1.9
- conv_value: bfloat16 [4096, 2048], P('sp', 'tp'), may hold values from -0.09375 to 0.09375
- conv_gate: bfloat16 [4096, 2048], P('sp', 'tp'), may hold values from -0.09375 to 0.09375
- state_feed: bfloat16 [4096, 2048], P('sp', 'tp'), may hold values from -0.09375 to 0.09375
- conv_taps: float32 [31, 2048], P(None, 'tp'), may hold values from -1 to 1
- chan_gain: float32 [2048], replicated, may hold values from 0.1 to 1.9
- chan_shift: float32 [2048], replicated, may hold values from -3 to 3
- conv_project: bfloat16 [2048, 4096], P('sp', 'tp'), may hold values from -0.125 to 0.125
- decay_rate: float32 [128, 64], P('tp'), may hold values from 0.1 to 3
- frequency: float32 [128, 64], P('tp'), may hold values from 0.1 to 3
- input_real: float32 [128, 64, 16], P('tp'), may hold values from -0.0390625 to 0.0390625
- input_imag: float32 [128, 64, 16], P('tp'), may hold values from -0.0390625 to 0.0390625
- output_real: float32 [128, 16, 64], P('tp'), may hold values from -0.5 to 0.5
- output_imag: float32 [128, 16, 64], P('tp'), may hold values from -0.5 to 0.5
- skip_gain: float32 [2048], P('tp'), may hold values from -3 to 3
- state_value: bfloat16 [2048, 4096], P('sp', 'tp'), may hold values from -0.125 to 0.125
- state_gate: bfloat16 [2048, 4096], P('sp', 'tp'), may hold values from -0.125 to 0.125
- initial_state: float32 [2, 128, 64], P(None, 'tp'), may hold values from -5 to 5
Outputs:
- mixer_out: bfloat16 [3072, 4096], P('sp', 'tp')
- final_state: float32 [2, 128, 64], P(None, 'tp')
All inputs are finite; a program needn't handle non-finite values.
Results may differ from a plain program's by a relative error of at most 0.0085.
Values may be sent and summed in bfloat16 or wider, within the bound.
A program may use at most 128 MiB of HBM per device.

v0:
```python
import functools
import jax
import jax.numpy as jnp
from jax import lax
from jax.experimental import pallas as pl
from jax.experimental.pallas import tpu as pltpu
from jax.sharding import PartitionSpec as P


def passed_along(value, axis, steps):
    count = lax.axis_size(axis)
    leading, last = (max(0, -steps), min(count, count - steps))
    return lax.ppermute(value, axis, [(source, source + steps) for source in range(leading, last)])


def rotate(first_real, first_imag, second_real, second_imag):
    return (
        first_real * second_real - first_imag * second_imag,
        first_real * second_imag + first_imag * second_real,
    )


def power_table(base_real, base_imag, exponent, largest):
    result_real = jnp.ones((exponent.shape[0], base_real.shape[0]), jnp.float32)
    result_imag = jnp.zeros((exponent.shape[0], base_real.shape[0]), jnp.float32)
    square_real, square_imag = (base_real, base_imag)
    for place in range(max(largest, 1).bit_length()):
        chosen = (exponent >> place & 1 == 1)[:, None]
        next_real, next_imag = rotate(result_real, result_imag, square_real, square_imag)
        result_real = jnp.where(chosen, next_real, result_real)
        result_imag = jnp.where(chosen, next_imag, result_imag)
        square_real, square_imag = rotate(square_real, square_imag, square_real, square_imag)
    return (result_real, result_imag)


def local(
    tokens,
    norm_gain,
    conv_value,
    conv_gate,
    state_feed,
    conv_taps,
    chan_gain,
    chan_shift,
    conv_project,
    decay_rate,
    frequency,
    input_real,
    input_imag,
    output_real,
    output_imag,
    skip_gain,
    state_value,
    state_gate,
    initial_state,
):
    highest = lax.Precision.HIGHEST
    floats = tokens.astype(jnp.float32)
    normed = (
        floats * lax.rsqrt(jnp.mean(floats * floats, axis=1, keepdims=True) + 1e-06) * norm_gain
    ).astype(jnp.bfloat16)
    length = tokens.shape[0]
    width = conv_value.shape[1]
    in_block = jnp.concatenate([conv_value, conv_gate, state_feed], axis=1)
    projected = jnp.dot(
        normed,
        lax.all_gather(in_block, "sp", axis=0, tiled=True),
        preferred_element_type=jnp.float32,
    )
    gated_linear = (projected[:, :width] * jax.nn.sigmoid(projected[:, width : 2 * width])).astype(
        jnp.bfloat16
    )
    state_drive = projected[:, 2 * width :].astype(jnp.bfloat16)
    kernel = conv_taps.shape[0]
    before = passed_along(gated_linear[length - (kernel - 1) :], "sp", 1)
    padded = jnp.concatenate([before, gated_linear], axis=0).astype(jnp.float32)
    conv_sum = jnp.zeros((length, width), jnp.float32)
    for offset in range(kernel):
        conv_sum = conv_sum + conv_taps[offset] * padded[offset : offset + length]
    conv_out = conv_sum.astype(jnp.bfloat16)
    seq_devices = lax.axis_size("sp")
    total_tokens = length * seq_devices
    groups, state_size, group_size = input_real.shape
    flat = groups * state_size
    rate_real = -decay_rate / total_tokens
    magnitude = jnp.exp(rate_real)
    step_real = magnitude * jnp.cos(frequency)
    step_imag = magnitude * jnp.sin(frequency)
    modulus = rate_real * rate_real + frequency * frequency
    lift_real = step_real - 1.0
    factor_real = (lift_real * rate_real + step_imag * frequency) / modulus
    factor_imag = (step_imag * rate_real - lift_real * frequency) / modulus
    drive_real = factor_real[..., None] * input_real - factor_imag[..., None] * input_imag
    drive_imag = factor_real[..., None] * input_imag + factor_imag[..., None] * input_real
    grouped = state_drive.astype(jnp.float32).reshape(length, groups, group_size)
    pushed_real = jnp.einsum("gph,tgh->tgp", drive_real, grouped, precision=highest).reshape(
        length, flat
    )
    pushed_imag = jnp.einsum("gph,tgh->tgp", drive_imag, grouped, precision=highest).reshape(
        length, flat
    )
    base_real = step_real.reshape(flat)
    base_imag = step_imag.reshape(flat)
    square_size = base_real * base_real + base_imag * base_imag
    back_real = base_real / square_size
    back_imag = -base_imag / square_size
    positions = lax.iota(jnp.int32, length)
    counted = positions + 1
    power_real, power_imag = power_table(base_real, base_imag, counted, length)
    undo_real, undo_imag = power_table(back_real, back_imag, counted, length)
    scaled_real, scaled_imag = rotate(undo_real, undo_imag, pushed_real, pushed_imag)
    lower = (positions[:, None] >= positions[None, :]).astype(jnp.float32)
    summed_real = jnp.dot(lower, scaled_real, precision=highest)
    summed_imag = jnp.dot(lower, scaled_imag, precision=highest)
    local_real, local_imag = rotate(power_real, power_imag, summed_real, summed_imag)
    span_real, span_imag = (power_real[-1], power_imag[-1])
    last_real, last_imag = (local_real[-1], local_imag[-1])
    start_real = initial_state[0].reshape(flat)
    start_imag = initial_state[1].reshape(flat)
    finals = lax.all_gather(jnp.stack([last_real, last_imag])[None], "sp", axis=0, tiled=True)
    position = lax.axis_index("sp")
    device_ids = lax.iota(jnp.int32, seq_devices)
    lag = jnp.maximum(position - 1 - device_ids, 0)
    weight_real, weight_imag = power_table(span_real, span_imag, lag, seq_devices)
    before_mask = (device_ids < position).astype(jnp.float32)[:, None]
    moved_real, moved_imag = rotate(weight_real, weight_imag, finals[:, 0], finals[:, 1])
    lead_real, lead_imag = power_table(
        span_real, span_imag, jnp.stack([position, jnp.int32(seq_devices)]), seq_devices
    )
    opening_real, opening_imag = rotate(lead_real[0], lead_imag[0], start_real, start_imag)
    entry_real = opening_real + jnp.sum(moved_real * before_mask, axis=0)
    entry_imag = opening_imag + jnp.sum(moved_imag * before_mask, axis=0)
    tail_real, tail_imag = power_table(
        span_real, span_imag, seq_devices - 1 - device_ids, seq_devices
    )
    carried_real, carried_imag = rotate(tail_real, tail_imag, finals[:, 0], finals[:, 1])
    closing_real, closing_imag = rotate(lead_real[1], lead_imag[1], start_real, start_imag)
    final_real = closing_real + jnp.sum(carried_real, axis=0)
    final_imag = closing_imag + jnp.sum(carried_imag, axis=0)
    final_state = jnp.stack([final_real, final_imag]).reshape(2, groups, state_size)
    state_real = (power_real * entry_real - power_imag * entry_imag + local_real).reshape(
        length, groups, state_size
    )
    state_imag = (power_real * entry_imag + power_imag * entry_real + local_imag).reshape(
        length, groups, state_size
    )
    response = jnp.einsum("ghp,tgp->tgh", output_real, state_real, precision=highest) - jnp.einsum(
        "ghp,tgp->tgh", output_imag, state_imag, precision=highest
    )
    response = response.reshape(length, groups * group_size) + skip_gain * state_drive.astype(
        jnp.float32
    )
    activated = jax.nn.gelu(response).astype(jnp.bfloat16)
    conv_rows, activated_rows = (
        lax.all_gather(conv_out, "tp", axis=1, tiled=True),
        lax.all_gather(activated, "tp", axis=1, tiled=True),
    )
    conv_full = conv_rows.astype(jnp.float32)
    row_mean = jnp.mean(conv_full, axis=1, keepdims=True)
    centred = conv_full - row_mean
    variance = jnp.mean(centred * centred, axis=1, keepdims=True)
    conv_act = jax.nn.silu(centred * lax.rsqrt(variance + 1e-05) * chan_gain + chan_shift).astype(
        jnp.bfloat16
    )
    columns = conv_project.shape[1]
    out_block = jnp.concatenate([conv_project, state_value, state_gate], axis=1)
    piece = lax.all_gather(out_block, "sp", axis=0, tiled=True)
    conv_branch = jnp.dot(conv_act, piece[:, :columns], preferred_element_type=jnp.float32)
    state_both = jnp.dot(activated_rows, piece[:, columns:], preferred_element_type=jnp.float32)
    mixer_out = (
        conv_branch + state_both[:, :columns] * jax.nn.sigmoid(state_both[:, columns:])
    ).astype(jnp.bfloat16)
    return (mixer_out, final_state)


def power_stack(base_real, base_imag, count):
    real, imag = (base_real[None], base_imag[None])
    while real.shape[0] < count:
        next_real, next_imag = rotate(real, imag, real[-1:], imag[-1:])
        real = jnp.concatenate([real, next_real], axis=0)
        imag = jnp.concatenate([imag, next_imag], axis=0)
    return (real[:count], imag[:count])


def block_diagonal(blocks):
    groups = blocks.shape[1]
    return blocks[:, :, :, None, :] * jnp.eye(groups, dtype=blocks.dtype)[None, :, None, :, None]


def chunk_matrices(decay_rate, frequency, input_real, input_imag, output_real, output_imag, total, chunk):
    highest = lax.Precision.HIGHEST
    groups, states, width = input_real.shape
    rate_real = -decay_rate / total
    magnitude = jnp.exp(rate_real)
    step_real = magnitude * jnp.cos(frequency)
    step_imag = magnitude * jnp.sin(frequency)
    modulus = rate_real * rate_real + frequency * frequency
    lift_real = step_real - 1.0
    factor_real = (lift_real * rate_real + step_imag * frequency) / modulus
    factor_imag = (step_imag * rate_real - lift_real * frequency) / modulus
    drive_real = factor_real[..., None] * input_real - factor_imag[..., None] * input_imag
    drive_imag = factor_real[..., None] * input_imag + factor_imag[..., None] * input_real
    power_real, power_imag = power_stack(step_real, step_imag, chunk)
    whole_real = jnp.concatenate([jnp.ones_like(step_real)[None], power_real], axis=0)
    whole_imag = jnp.concatenate([jnp.zeros_like(step_imag)[None], power_imag], axis=0)
    back_real = whole_real[:chunk][::-1, :, :, None]
    back_imag = whole_imag[:chunk][::-1, :, :, None]
    push_real, push_imag = rotate(back_real, back_imag, drive_real[None], drive_imag[None])
    push = [
        block_diagonal(value.transpose(0, 1, 3, 2)).reshape(chunk * groups * width, groups * states)
        for value in (push_real, push_imag)
    ]
    push = jnp.concatenate(push, axis=1)
    out_real, out_imag = rotate(
        output_real[None], output_imag[None], whole_real[:, :, None, :], whole_imag[:, :, None, :]
    )
    emit = [
        block_diagonal(value.transpose(1, 3, 0, 2).reshape(1, groups, states, chunk * width))
        for value in (out_real[1:], -out_imag[1:])
    ]
    emit = [
        value.reshape(groups, states, groups, chunk, width)
        .transpose(0, 1, 3, 2, 4)
        .reshape(groups * states, chunk * groups * width)
        for value in emit
    ]
    emit = jnp.concatenate(emit, axis=0)
    response = jnp.einsum(
        "dghp,gpi->dgih", out_real[:chunk], drive_real, precision=highest
    ) - jnp.einsum("dghp,gpi->dgih", out_imag[:chunk], drive_imag, precision=highest)
    spread = block_diagonal(response).reshape(chunk, groups * width, groups * width)
    spread = spread.transpose(1, 0, 2).reshape(groups * width, chunk * groups * width)
    padded = jnp.concatenate([jnp.zeros_like(spread), spread], axis=1)
    span = groups * width
    full = chunk * span
    inside = jnp.concatenate(
        [padded[:, full - place * span : 2 * full - place * span] for place in range(chunk)], axis=0
    )
    return (power_real[-1].reshape(-1), power_imag[-1].reshape(-1), push, emit, inside)


def recurrence(feed, skip_gain, start, matrices, chunk):
    highest = lax.Precision.HIGHEST
    span_real, span_imag, push, emit, inside = matrices
    length, width = feed.shape
    count = length // chunk
    rows = feed.reshape(count, chunk * width).astype(jnp.float32)
    pushed = jnp.dot(rows, push, precision=highest)
    flat = span_real.shape[0]
    first_real, first_imag = rotate(span_real, span_imag, start[0], start[1])
    head = jnp.concatenate([first_real, first_imag])[None]
    pushed = jnp.concatenate([pushed[:1] + head, pushed[1:]], axis=0)
    real, imag = (pushed[:, :flat], pushed[:, flat:])
    shift = 1
    while shift < count:
        moved_real = jnp.pad(real[:-shift], ((shift, 0), (0, 0)))
        moved_imag = jnp.pad(imag[:-shift], ((shift, 0), (0, 0)))
        add_real, add_imag = rotate(span_real, span_imag, moved_real, moved_imag)
        real, imag = (real + add_real, imag + add_imag)
        span_real, span_imag = rotate(span_real, span_imag, span_real, span_imag)
        shift *= 2
    entry_real = jnp.concatenate([start[0][None], real[:-1]], axis=0)
    entry_imag = jnp.concatenate([start[1][None], imag[:-1]], axis=0)
    entry = jnp.concatenate([entry_real, entry_imag], axis=1)
    response = jnp.dot(rows, inside, precision=highest) + jnp.dot(entry, emit, precision=highest)
    response = response + jnp.tile(skip_gain, chunk) * rows
    activated = jax.nn.gelu(response).astype(jnp.bfloat16).reshape(length, width)
    return (activated, jnp.stack([real[-1], imag[-1]]))


def remote(source, target, send_sem, recv_sem, device):
    return pltpu.make_async_remote_copy(
        src_ref=source,
        dst_ref=target,
        send_sem=send_sem,
        recv_sem=recv_sem,
        device_id=device,
        device_id_type=pl.DeviceIdType.MESH,
    )


def plane_neighbours(inner, core):
    flip_x = inner + 1 - 2 * (inner % 2)
    flip_y = inner + 2 - 4 * (inner // 2)
    first = flip_x * (1 - core) + flip_y * core
    second = flip_y * (1 - core) + flip_x * core
    return (first, second, 3 - inner)


def entry_kernel(
    depth, own_ref, in_ref, project_ref, value_ref, gate_ref, all_ref, taken_ref, moved_ref, sent,
    landed, in_sent, in_landed, out_sent, out_landed, local_sem
):
    outer, inner, core = (lax.axis_index("outer"), lax.axis_index("inner"), lax.axis_index("tp"))
    first, second, opposite = plane_neighbours(inner, core)
    length = own_ref.shape[0]
    devices = 4 * depth
    here = outer * 4 + inner
    half = devices // 2
    target_core = here // half

    def slot(index):
        return all_ref.at[pl.ds(pl.multiple_of(index * length, length), length)]

    def send(index, lane, device, source=None):
        return remote(
            slot(index) if source is None else source,
            slot(index),
            sent.at[index, lane],
            landed.at[index],
            device,
        )

    def arrived(index):
        send(index, 0, (outer, first, core)).wait_recv()

    def spread(index, source=None):
        send(index, 0, (outer, first, core), source).start()
        send(index, 1, (outer, second, core), source).start()

    up, down = ((outer + 1, inner, core), (outer - 1, inner, core))

    @pl.when(outer < depth - 1)
    def _():
        send(here, 2, up, own_ref).start()

    @pl.when(outer > 0)
    def _():
        send(here, 3, down, own_ref).start()

    spread(here, own_ref)
    keep = pltpu.make_async_copy(own_ref, slot(here), local_sem.at[0])
    keep.start()
    place = core * half + here % half

    def in_copy(offset):
        other = (here + offset) % devices
        return remote(
            in_ref.at[other],
            taken_ref.at[place],
            in_sent.at[offset],
            in_landed.at[place],
            (other // 4, other % 4, target_core),
        )

    in_keep = pltpu.make_async_copy(in_ref.at[here], taken_ref.at[place], local_sem.at[1])

    @pl.when(core == target_core)
    def _():
        in_keep.start()

    @pl.when(core != target_core)
    def _():
        in_copy(0).start()

    for offset in range(1, devices):
        in_copy(offset).start()

    out_refs = (project_ref, value_ref, gate_ref)
    out_rows, columns = project_ref.shape
    piece = columns // 4

    def out_from(which, other):
        return out_refs[which].at[:, pl.ds(pl.multiple_of(other * piece, piece), piece)]

    def out_to(which, origin):
        rows = pl.ds(pl.multiple_of(origin * out_rows, out_rows), out_rows)
        return moved_ref.at[rows, pl.ds(which * piece, piece)]

    def out_keep(which):
        return pltpu.make_async_copy(
            out_from(which, inner), out_to(which, inner), local_sem.at[2 + which]
        )

    def out_copy(which, offset):
        other = (inner + offset) % 4
        return remote(
            out_from(which, other),
            out_to(which, inner),
            out_sent.at[which, offset],
            out_landed.at[which, inner],
            (outer, other, core),
        )

    for which in range(3):
        out_keep(which).start()
        for offset in range(1, 4):
            out_copy(which, offset).start()

    def side(z):
        index = z * 4 + first
        arrived(index)
        send(index, 1, (outer, second, core)).start()

    side(outer)
    for step in range(1, depth):
        below, above = (outer - step, outer + step)

        @pl.when(below >= 0)
        def _():
            index = below * 4 + inner
            arrived(index)

            @pl.when(outer < depth - 1)
            def _():
                send(index, 2, up).start()

            spread(index)

        @pl.when(above < depth)
        def _():
            index = above * 4 + inner
            arrived(index)

            @pl.when(outer > 0)
            def _():
                send(index, 3, down).start()

            spread(index)

        @pl.when(below >= 0)
        def _():
            side(below)

        @pl.when(above < depth)
        def _():
            side(above)

    for z in range(depth):
        arrived(z * 4 + second)
        arrived(z * 4 + opposite)

    for z in range(depth):
        index = z * 4 + inner
        send(index, 0, (outer, first, core)).wait_send()
        send(index, 1, (outer, second, core)).wait_send()
        send(z * 4 + first, 1, (outer, second, core)).wait_send()

        @pl.when(jnp.logical_and(outer < depth - 1, z <= outer))
        def _():
            send(index, 2, up).wait_send()

        @pl.when(jnp.logical_and(outer > 0, z >= outer))
        def _():
            send(index, 3, down).wait_send()

    keep.wait()

    @pl.when(core == target_core)
    def _():
        in_keep.wait()

    @pl.when(core != target_core)
    def _():
        in_copy(0).wait_send()

    for offset in range(1, devices):
        in_copy(offset).wait_send()

    def in_wait(index):
        remote(
            in_ref.at[0],
            taken_ref.at[index],
            in_sent.at[0],
            in_landed.at[index],
            (outer, first, core),
        ).wait_recv()

    for lane in range(2):
        for index in range(half):
            local_one = jnp.logical_and(here == core * half + index, core == lane)

            @pl.when(jnp.logical_not(local_one))
            def _():
                in_wait(lane * half + index)

    for which in range(3):
        out_keep(which).wait()
        for offset in range(1, 4):
            out_copy(which, offset).wait_send()
        for offset in range(1, 4):
            other = (inner + offset) % 4
            remote(
                out_from(which, other),
                out_to(which, other),
                out_sent.at[which, 0],
                out_landed.at[which, other],
                (outer, first, core),
            ).wait_recv()


def entry_exchange(own_half, in_block, out_weights, depth):
    devices = 4 * depth
    length, half = own_half.shape
    out_rows, columns = out_weights[0].shape
    any_spec = pl.BlockSpec(memory_space=pl.ANY)
    dma = pltpu.SemaphoreType.DMA
    return pl.pallas_call(
        functools.partial(entry_kernel, depth),
        out_shape=(
            jax.ShapeDtypeStruct((devices * length, half), own_half.dtype),
            jax.ShapeDtypeStruct(in_block.shape, in_block.dtype),
            jax.ShapeDtypeStruct((4 * out_rows, 3 * (columns // 4)), in_block.dtype),
        ),
        in_specs=[any_spec] * 5,
        out_specs=(any_spec,) * 3,
        scratch_shapes=[
            dma((devices, 4)),
            dma((devices,)),
            dma((devices,)),
            dma((devices,)),
            dma((3, 4)),
            dma((3, 4)),
            dma((5,)),
        ],
        compiler_params=pltpu.CompilerParams(has_side_effects=True),
        cost_estimate=pl.CostEstimate(flops=0, bytes_accessed=0, transcendentals=0),
    )(own_half, in_block, *out_weights)


def middle_kernel(depth, mixed_ref, last_ref, turned_ref, states_ref, sent, landed, last_sent, last_landed, local_sem):
    outer, inner, core = (lax.axis_index("outer"), lax.axis_index("inner"), lax.axis_index("tp"))
    devices = 4 * depth
    here = outer * 4 + inner
    keep = pltpu.make_async_copy(mixed_ref.at[here], turned_ref.at[here], local_sem.at[0])
    keep_last = pltpu.make_async_copy(last_ref, states_ref.at[here], local_sem.at[1])
    keep.start()
    keep_last.start()

    def copies(offset):
        other = (here + offset) % devices
        device = (other // 4, other % 4, core)
        return (
            remote(
                mixed_ref.at[other], turned_ref.at[here], sent.at[offset], landed.at[here], device
            ),
            remote(
                last_ref, states_ref.at[here], last_sent.at[offset], last_landed.at[here], device
            ),
        )

    for offset in range(1, devices):
        for copy in copies(offset):
            copy.start()
    keep.wait()
    keep_last.wait()
    for offset in range(1, devices):
        for copy in copies(offset):
            copy.wait_send()
    for offset in range(1, devices):
        other = (here + offset) % devices
        device = (other // 4, other % 4, core)
        remote(
            mixed_ref.at[other], turned_ref.at[other], sent.at[offset], landed.at[other], device
        ).wait_recv()
        remote(
            last_ref, states_ref.at[other], last_sent.at[offset], last_landed.at[other], device
        ).wait_recv()


def middle_exchange(mixed, last, depth):
    devices = 4 * depth
    any_spec = pl.BlockSpec(memory_space=pl.ANY)
    dma = pltpu.SemaphoreType.DMA
    return pl.pallas_call(
        functools.partial(middle_kernel, depth),
        out_shape=(
            jax.ShapeDtypeStruct(mixed.shape, mixed.dtype),
            jax.ShapeDtypeStruct((devices,) + last.shape, last.dtype),
        ),
        in_specs=[any_spec] * 2,
        out_specs=(any_spec,) * 2,
        scratch_shapes=[dma((devices,))] * 4 + [dma((2,))],
        compiler_params=pltpu.CompilerParams(has_side_effects=True),
    )(mixed, last)


def exit_kernel(own_ref, all_ref, sent, landed, local_sem):
    outer, inner, core = (lax.axis_index("outer"), lax.axis_index("inner"), lax.axis_index("tp"))
    first, second, opposite = plane_neighbours(inner, core)
    length, half = own_ref.shape[1:]

    def slot(index, side):
        rows = pl.ds(pl.multiple_of(index * length, length), length)
        return all_ref.at[:, rows, pl.ds(pl.multiple_of(side * half, half), half)]

    def send(index, lane, device, source=None):
        return remote(
            slot(index, core) if source is None else source,
            slot(index, core),
            sent.at[index, lane],
            landed.at[core, index],
            device,
        )

    peer = (outer, inner, 1 - core)
    near, far = ((outer, first, core), (outer, second, core))
    send(inner, 0, near, own_ref).start()
    send(inner, 1, far, own_ref).start()
    send(inner, 2, peer, own_ref).start()
    keep = pltpu.make_async_copy(own_ref, slot(inner, core), local_sem.at[0])
    keep.start()
    send(first, 0, near).wait_recv()
    send(first, 1, far).start()
    send(first, 2, peer).start()
    for index in (second, opposite):
        send(index, 0, near).wait_recv()
        send(index, 2, peer).start()
    for index in range(4):
        remote(
            own_ref,
            slot(index, 1 - core),
            sent.at[index, 2],
            landed.at[1 - core, index],
            peer,
        ).wait_recv()
    send(inner, 0, near).wait_send()
    send(inner, 1, far).wait_send()
    send(first, 1, far).wait_send()
    for index in (inner, first, second, opposite):
        send(index, 2, peer).wait_send()
    keep.wait()


def exit_gather(both):
    parts, length, half = both.shape
    any_spec = pl.BlockSpec(memory_space=pl.ANY)
    dma = pltpu.SemaphoreType.DMA
    return pl.pallas_call(
        exit_kernel,
        out_shape=jax.ShapeDtypeStruct((parts, 4 * length, 2 * half), both.dtype),
        in_specs=[any_spec],
        out_specs=any_spec,
        scratch_shapes=[dma((4, 3)), dma((2, 4)), dma((1,))],
        compiler_params=pltpu.CompilerParams(has_side_effects=True),
    )(both)


def channel_local(
    tokens,
    norm_gain,
    conv_value,
    conv_gate,
    state_feed,
    conv_taps,
    chan_gain,
    chan_shift,
    conv_project,
    decay_rate,
    frequency,
    input_real,
    input_imag,
    output_real,
    output_imag,
    skip_gain,
    state_value,
    state_gate,
    initial_state,
):
    seq = ("outer", "inner")
    devices = lax.axis_size("outer") * lax.axis_size("inner")
    inner = lax.axis_size("inner")
    position = lax.axis_index("outer") * inner + lax.axis_index("inner")
    core = lax.axis_index("tp")
    swap = [(0, 1), (1, 0)]
    local_length, model = tokens.shape
    total = local_length * devices
    half = model // 2
    floats = tokens.astype(jnp.float32)
    normed = (
        floats * lax.rsqrt(jnp.mean(floats * floats, axis=1, keepdims=True) + 1e-06) * norm_gain
    ).astype(jnp.bfloat16)
    own_half = lax.dynamic_slice_in_dim(normed, core * half, half, axis=1)
    rows, wide = conv_value.shape
    share = wide // devices
    in_block = jnp.concatenate(
        [weight.T.reshape(devices, share, rows) for weight in (conv_value, conv_gate, state_feed)],
        axis=1,
    )
    out_rows, columns = conv_project.shape
    piece = columns // inner
    all_half, in_block, out_block = entry_exchange(
        own_half, in_block, (conv_project, state_value, state_gate), lax.axis_size("outer")
    )
    in_block = in_block.reshape(2, devices // 2, 3 * share, rows).transpose(0, 2, 1, 3)
    in_block = in_block.reshape(6 * share, half)
    out_block = lax.all_gather(out_block, "outer", axis=0, tiled=True)
    groups = decay_rate.shape[0] // devices
    chunk = 8

    def own(value, axis=0, size=groups):
        return lax.dynamic_slice_in_dim(value, position * size, size, axis=axis)

    matrices = chunk_matrices(
        own(decay_rate),
        own(frequency),
        own(input_real),
        own(input_imag),
        own(output_real),
        own(output_imag),
        total,
        chunk,
    )
    partial = lax.dot_general(
        in_block, all_half, (((1,), (1,)), ((), ())), preferred_element_type=jnp.float32
    ).reshape(2, 3 * share, total)
    other = lax.dynamic_index_in_dim(partial, 1 - core, axis=0, keepdims=False)
    kept = lax.dynamic_index_in_dim(partial, core, axis=0, keepdims=False)
    projected = (kept + lax.ppermute(other, "tp", swap)).T
    gated = (projected[:, :share] * jax.nn.sigmoid(projected[:, share : 2 * share])).astype(
        jnp.bfloat16
    )
    feed = projected[:, 2 * share :].astype(jnp.bfloat16)
    kernel = conv_taps.shape[0]
    taps = own(conv_taps, 1, share)
    padded = jnp.pad(gated, ((kernel - 1, 0), (0, 0))).astype(jnp.float32)
    conv_sum = jnp.zeros((total, share), jnp.float32)
    for offset in range(kernel):
        conv_sum = conv_sum + taps[offset] * padded[offset : offset + total]
    conv_out = conv_sum.astype(jnp.bfloat16)
    start = own(initial_state, 1).reshape(2, -1)
    activated, last = recurrence(feed, own(skip_gain, 0, share), start, matrices, chunk)
    states = initial_state.shape[2]
    mixed = jnp.concatenate([conv_out, activated], axis=1).reshape(devices, local_length, 2 * share)
    mixed, last = middle_exchange(mixed, last.reshape(-1, 128), lax.axis_size("outer"))
    mixed = mixed.transpose(1, 0, 2)
    final_state = last.reshape(devices, 2, groups, states).transpose(1, 0, 2, 3)
    final_state = final_state.reshape(initial_state.shape)
    conv_full = mixed[:, :, :share].reshape(local_length, wide).astype(jnp.float32)
    active = mixed[:, :, share:].reshape(local_length, wide)
    own_mean = jnp.mean(conv_full, axis=1, keepdims=True)
    deviation = conv_full - own_mean
    own_spread = jnp.mean(deviation * deviation, axis=1, keepdims=True)
    peer = lax.ppermute(jnp.concatenate([own_mean, own_spread], axis=1), "tp", swap)
    row_mean = 0.5 * (own_mean + peer[:, :1])
    gap = 0.5 * (own_mean - peer[:, :1])
    variance = 0.5 * (own_spread + peer[:, 1:]) + gap * gap
    gain = lax.dynamic_slice_in_dim(chan_gain, core * wide, wide, axis=0)
    bias = lax.dynamic_slice_in_dim(chan_shift, core * wide, wide, axis=0)
    conv_act = jax.nn.silu(
        (conv_full - row_mean) * lax.rsqrt(variance + 1e-05) * gain + bias
    ).astype(jnp.bfloat16)
    both = jnp.stack([conv_act, active], axis=0)
    both = exit_gather(both)
    conv_branch = jnp.dot(both[0], out_block[:, :piece], preferred_element_type=jnp.float32)
    state_both = jnp.dot(both[1], out_block[:, piece:], preferred_element_type=jnp.float32)
    mixer = (conv_branch + state_both[:, :piece] * jax.nn.sigmoid(state_both[:, piece:])).astype(
        jnp.bfloat16
    )
    mixer = mixer.reshape(inner, local_length, piece)
    mixer = lax.all_to_all(mixer, "inner", 0, 0, tiled=True)
    mixer_out = mixer.transpose(1, 0, 2).reshape(local_length, columns)
    return (mixer_out, final_state)


def specs_of(seq):
    in_specs = (
        P(seq, None),
        P(),
        P(seq, "tp"),
        P(seq, "tp"),
        P(seq, "tp"),
        P(None, "tp"),
        P(),
        P(),
        P(seq, "tp"),
        P("tp", None),
        P("tp", None),
        P("tp", None, None),
        P("tp", None, None),
        P("tp", None, None),
        P("tp", None, None),
        P("tp"),
        P(seq, "tp"),
        P(seq, "tp"),
        P(None, "tp", None),
    )
    return (in_specs, (P(seq, "tp"), P(None, "tp", None)))


def solution(mesh):
    seq_devices, cores = (mesh.shape["sp"], mesh.shape["tp"])
    fine = jax.sharding.Mesh(
        mesh.devices.reshape(seq_devices // 4, 4, cores), ("outer", "inner", "tp")
    )

    def run(*args):
        groups = args[9].shape[0]
        if cores == 2 and groups % (cores * seq_devices) == 0:
            in_specs, out_specs = specs_of(("outer", "inner"))
            body = jax.shard_map(
                channel_local, mesh=fine, in_specs=in_specs, out_specs=out_specs, check_vma=False
            )
        else:
            in_specs, out_specs = specs_of("sp")
            body = jax.shard_map(
                local, mesh=mesh, in_specs=in_specs, out_specs=out_specs, check_vma=False
            )
        return body(*args)

    return run
```

profile of v0, /device:TPU:0, one launch (start us, length us, event | category | flops | bytes accessed | tf_op | source)
XLA Modules:
  0.0 368.8 jit_solution(16140230743303860905)
XLA Ops:
  7.2 1.9 convert_element_type.98
  9.5 2.1 copy.34
  11.6 2.0 copy.35
  13.6 2.0 copy.36
  15.7 1.1 fusion.17.own_ref
  17.3 1.2 pad_maximum_fusion.in_ref
  18.5 146.5 %shard_map.194 = (bf16[3072,2048]{1,0:T(8,128)(2,1)}, bf16[16,192,256]{2,1,0:T(8,128)(2,1)}, bf16[512,1536]{1,0:T(8,128)(2,1)}) custom-call(bf16[192,2048]{1,0:T(8,128)(2,1)} %fusion.17.own_ref, bf16[16,192,256]{2,1,0:T(8,128)(2,1)} %pad_maximum_fusion.in_ref, bf16[128,2048]{1,0:T(8,128)(2,1)} %project_ref.1, bf16[128,2048]{1,0:T(8,128)(2,1)} %value_ref.1, ...), custom_call_target="tpu_custom_call" | custom-call | tf_op jit(solution)/shard_map/pallas_call | solution.py:498
  165.0 1.6 copy.55
  166.7 10.2 %fusion = f32[2,192,3072]{2,1,0:T(8,128)} fusion(bf16[2,192,2048]{2,1,0:T(8,128)(2,1)S(1)} %bitcast.171, bf16[3072,2048]{1,0:T(8,128)(2,1)} %get-tuple-element.8), kind=kOutput, calls=%fused_computation | convolution fusion | flops 4831838208 | bytes 18874368 | tf_op jit(solution)/shard_map/dot_general | solution.py:704
  176.9 3.3 dynamic-slice_bitcast_fusion
  180.1 3.2 collective-permute-start
  183.4 0.8 fusion.124
  184.2 0.7 subtract_divide_fusion
  185.0 0.7 constant_dynamic-slice_fusion.2
  185.8 0.6 slice.449
  186.5 0.7 slice.478
  187.3 0.8 fusion.118
  188.8 1.4 mul.1884
  190.2 1.4 mul.1889
  191.8 0.8 constant_dynamic-slice_fusion.3
  193.7 1.4 mul.1975
  195.1 1.4 mul.1978
  196.5 2.7 fusion.107
  199.2 2.7 fusion.24
  203.1 0.8 dynamic_slice.54
  203.9 0.6 mul.1979
  204.6 1.7 dynamic-slice_bitcast_fusion.30
  206.2 2.0 fusion.128
  208.2 0.6 multiply_subtract_fusion.7
  210.9 2.6 fusion.9
  214.4 2.1 fusion.25
  220.1 0.8 copy-done.8
  221.6 2.3 fusion.131
  224.0 3.8 %fusion.41 = bf16[384,512]{1,0:T(8,128)(2,1)} fusion(f32[384,512]{1,0:T(8,128)S(1)} %fusion.131, f32[256,512]{0,1:T(8,128)} %mul.1978, f32[256,512]{0,1:T(8,128)S(1)} %copy-done.7, f32[383,256]{1,0:T(8,128)} %bitcast.178, f32[1,256]{1,0:T(1,128)S(1)} %copy-done.60, f32[383,256]{1,0:T(8,128)} %bitcast.177, f32[1,256]{1,0:T(1,128)S(1)} %copy-done.59, ...), kind=kOutput, calls=%fused_computation.48 | convolution fusion | flops 1211367424 | bytes 3409920 | tf_op jit(solution)/shard_map/dot_general | solution.py:265
  228.1 1.5 concatenate.80
  230.4 7.3 %fusion.45 = bf16[3072,64]{0,1:T(8,128)(2,1)S(1)} fusion(f32[3102,64]{0,1:T(8,128)S(1)} %pad_convert_fusion, f32[64]{0:T(128)S(1)} %copy-done.57, f32[64]{0:T(128)S(1)} %copy-done.28, f32[64]{0:T(128)S(1)} %copy-done.29, f32[64]{0:T(128)S(1)} %copy-done.30, f32[64]{0:T(128)S(1)} %copy-done.31, f32[64]{0:T(128)S(1)} %copy-done.32, f32[64]{0:T(128)S(1)} %copy-done.33, ...), kind=kLoop, calls=%fused_computation.53 | loop fusion | flops 12189696 | bytes 24780544 | tf_op jit(solution)/shard_map/convert_element_type | solution.py:720
  238.1 1.3 pad_maximum_fusion.1.mixed_ref
  239.4 32.5 %shard_map.195 = (bf16[16,192,128]{2,1,0:T(8,128)(2,1)}, f32[16,4,128]{2,1,0:T(4,128)}) custom-call(bf16[16,192,128]{2,1,0:T(8,128)(2,1)} %pad_maximum_fusion.1.mixed_ref, f32[4,128]{1,0:T(4,128)} %reshape.502.last_ref), custom_call_target="tpu_custom_call" | custom-call | tf_op jit(solution)/shard_map/pallas_call | solution.py:565
  272.0 1.4 fusion.87
  273.4 1.5 multiply_reduce_fusion.1
  277.4 0.9 pad_maximum_fusion.2.own_ref
  278.3 56.5 %shard_map.196 = bf16[2,768,2048]{2,1,0:T(8,128)(2,1)} custom-call(bf16[2,192,1024]{2,1,0:T(8,128)(2,1)} %pad_maximum_fusion.2.own_ref), custom_call_target="tpu_custom_call" | custom-call | tf_op jit(solution)/shard_map/pallas_call | solution.py:629
  334.9 6.6 %fusion.2 = f32[768,1024]{1,0:T(8,128)S(1)} fusion(bf16[2048,1536]{1,0:T(8,128)(2,1)} %all-gather.2.cloned.1.call-done, bf16[2,768,2048]{2,1,0:T(8,128)(2,1)} %shard_map.196), kind=kOutput, calls=%fused_computation.2 | convolution fusion | flops 3221225472 | bytes 10485760 | tf_op jit(solution)/shard_map/dot_general | solution.py:746
  341.5 4.4 %fusion.18 = bf16[768,512]{1,0:T(8,128)(2,1)} fusion(f32[768,1024]{1,0:T(8,128)S(1)} %fusion.2, bf16[2048,1536]{1,0:T(8,128)(2,1)} %all-gather.2.cloned.1.call-done, bf16[2,768,2048]{2,1,0:T(8,128)(2,1)S(1)} %copy-done.1), kind=kOutput, calls=%fused_computation.25 | convolution fusion | flops 1612972032 | bytes 9175040 | tf_op jit(solution)/shard_map/dot_general | solution.py:745
  345.9 3.5 all-to-all-start
  349.5 0.6 copy.52
  350.1 10.9 %all-to-all-done = bf16[4,192,512]{2,1,0:T(8,128)(2,1)S(1)} async-done(((bf16[4,192,512]{2,1,0:T(8,128)(2,1)}), bf16[4,192,512]{2,1,0:T(8,128)(2,1)S(1)}, u32[]{:S(2)}, u32[]{:S(2)}) %all-to-all-start) | async-done | bytes 786464 | tf_op jit(solution)/shard_map/all_to_all | solution.py:751
  361.0 1.0 copy.56
  (227 shorter events, 14.6 us)
Async XLA Ops:
  7.2 327.7 %all-gather.2.cloned.1.call-start = ((), (), s32[]{:S(2)}) async-start(), calls=%async_computation.1 | async-start | bytes 7864320 | tf_op jit(solution)/shard_map/all_gather | solution.py:687
  7.2 1.9 copy-start.2
  9.1 6.6 %copy-start.26 = (f32[4096]{0:T(1024)S(1)}, f32[4096]{0:T(1024)}, u32[]{:S(2)}) copy-start(f32[4096]{0:T(1024)} %param.20) | copy-start | bytes 49156
  15.7 1.1 copy-start.3
  15.7 1.3 copy-start.4
  15.7 1.6 copy-start.5
  180.1 30.8 %collective-permute-start = (f32[192,3072]{1,0:T(8,128)}, f32[192,3072]{1,0:T(8,128)}, u32[]{:S(2)}, u32[]{:S(2)}) collective-permute-start(f32[192,3072]{1,0:T(8,128)} %dynamic-slice_bitcast_fusion), channel_id=1, source_target_pairs={{0,1},{1,0},{2,3},{3,2},{4,5},{5,4},{6,7},{7,6},{8,9},{9,8},{10,11... | collective-permute-start | bytes 7077896 | tf_op jit(solution)/shard_map/ppermute | solution.py:709
  214.4 2.2 copy-start.11
  219.5 4.5 %copy-start.7 = (f32[256,512]{0,1:T(8,128)S(1)}, f32[256,512]{0,1:T(8,128)}, u32[]{:S(2)}) copy-start(f32[256,512]{0,1:T(8,128)} %mul.1975) | copy-start | bytes 1572868
  219.5 4.5 %copy-start.58 = (f32[512]{0:T(512)S(1)}, f32[512]{0:T(512)}, u32[]{:S(2)}) copy-start(f32[512]{0:T(512)} %mul.1979) | copy-start | bytes 6148
  219.5 4.5 %copy-start.59 = (f32[1,256]{1,0:T(1,128)S(1)}, f32[1,256]{1,0:T(1,128)}, u32[]{:S(2)}) copy-start(f32[1,256]{1,0:T(1,128)} %slice.449) | copy-start | bytes 3076
  219.5 4.5 %copy-start.60 = (f32[1,256]{1,0:T(1,128)S(1)}, f32[1,256]{1,0:T(1,128)}, u32[]{:S(2)}) copy-start(f32[1,256]{1,0:T(1,128)} %slice.478) | copy-start | bytes 3076
  227.8 2.2 copy-start.27
  227.8 2.2 copy-start.28
  227.8 2.2 copy-start.29
  227.8 2.3 copy-start.30
  227.8 2.3 copy-start.31
  227.8 2.3 copy-start.32
  227.9 2.3 copy-start.33
  227.9 2.3 copy-start.34
  227.9 2.3 copy-start.35
  227.9 2.3 copy-start.36
  227.9 2.3 copy-start.37
  227.9 2.3 copy-start.38
  227.9 2.3 copy-start.39
  227.9 2.3 copy-start.40
  227.9 2.3 copy-start.41
  227.9 2.3 copy-start.42
  228.0 2.3 copy-start.43
  228.0 2.3 copy-start.44
  228.0 2.3 copy-start.45
  228.0 2.3 copy-start.46
  228.0 2.3 copy-start.47
  228.0 2.3 copy-start.48
  228.0 2.3 copy-start.49
  228.0 2.3 copy-start.50
  228.0 2.3 copy-start.51
  228.0 2.3 copy-start.52
  228.1 2.3 copy-start.53
  228.1 2.3 copy-start.54
  228.1 2.3 copy-start.55
  228.1 2.3 copy-start.56
  228.1 2.3 copy-start.57
  272.0 3.1 copy-start
  275.0 2.0 collective-permute-start.1
  334.9 6.6 %copy-start.1 = (bf16[2,768,2048]{2,1,0:T(8,128)(2,1)S(1)}, bf16[2,768,2048]{2,1,0:T(8,128)(2,1)}, u32[]{:S(2)}) copy-start(bf16[2,768,2048]{2,1,0:T(8,128)(2,1)} %shard_map.196) | copy-start | bytes 18874372
  341.5 7.9 %copy-start.10 = (f32[16,4,128]{2,1,0:T(4,128)S(1)}, f32[16,4,128]{2,1,0:T(4,128)}, u32[]{:S(2)}) copy-start(f32[16,4,128]{2,1,0:T(4,128)} %get-tuple-element.11) | copy-start | bytes 98308
  345.9 15.1 %all-to-all-start = ((bf16[4,192,512]{2,1,0:T(8,128)(2,1)}), bf16[4,192,512]{2,1,0:T(8,128)(2,1)S(1)}, u32[]{:S(2)}, u32[]{:S(2)}) async-start(bf16[4,192,512]{2,1,0:T(8,128)(2,1)} %bitcast.70), calls=%async_computation | async-start | bytes 1572864 | tf_op jit(solution)/shard_map/all_to_all | solution.py:751
  (19 other events, 14.2 us)
Sparse Core Ops, SparseCore 0:
  183.5 132.3 all-gather.1
where the time goes:
time: 370 us; the launch traced here: 369 us
  Pallas kernels  236 us (64%)
  local copies, waits for them, and re-layouts  37.4 us (10%)
  matrix products  34.9 us (9%)
  other arithmetic  27.8 us (8%)
  between operations  15.5 us (4%)
  waiting for transfers between devices  10.9 us (3%)
  starting transfers between devices  6.81 us (2%)
    pallas_call x1, Pallas kernels, entry_exchange(): pl.pallas_call(functools.partial(entry_kernel, depth), out_shape=(jax.Sha...  146 us
    pallas_call x1, Pallas kernels, exit_gather(): pl.pallas_call(exit_kernel, out_shape=jax.ShapeDtypeStruct((parts, 4 * le...  56.5 us
    pallas_call x1, Pallas kernels, middle_exchange(): pl.pallas_call(functools.partial(middle_kernel, depth), out_shape=(jax.Sh...  32.5 us
    all_to_all x1, waiting for transfers between devices, channel_local(): mixer = lax.all_to_all(mixer, 'inner', 0, 0, tiled=True)  10.9 us
    dot_general x1, matrix products, channel_local(): lax.dot_general(in_block, all_half, (((1,), (1,)), ((), ())), preferred_e...  10.2 us
  transfers between devices with their start and end apart: 4, of which 1 were waited for; matrix products, arithmetic and copies ran while one was open for 16% of the time, Pallas kernels for 24%

commit v1 on v0

v1 whole, which is shorter than its diff:
```python
import functools
import jax
import jax.numpy as jnp
from jax import lax
from jax.experimental import pallas as pl
from jax.experimental.pallas import tpu as pltpu
from jax.sharding import PartitionSpec as P


def passed_along(value, axis, steps):
    count = lax.axis_size(axis)
    leading, last = (max(0, -steps), min(count, count - steps))
    return lax.ppermute(value, axis, [(source, source + steps) for source in range(leading, last)])


def rotate(first_real, first_imag, second_real, second_imag):
    return (
        first_real * second_real - first_imag * second_imag,
        first_real * second_imag + first_imag * second_real,
    )


def power_table(base_real, base_imag, exponent, largest):
    result_real = jnp.ones((exponent.shape[0], base_real.shape[0]), jnp.float32)
    result_imag = jnp.zeros((exponent.shape[0], base_real.shape[0]), jnp.float32)
    square_real, square_imag = (base_real, base_imag)
    for place in range(max(largest, 1).bit_length()):
        chosen = (exponent >> place & 1 == 1)[:, None]
        next_real, next_imag = rotate(result_real, result_imag, square_real, square_imag)
        result_real = jnp.where(chosen, next_real, result_real)
        result_imag = jnp.where(chosen, next_imag, result_imag)
        square_real, square_imag = rotate(square_real, square_imag, square_real, square_imag)
    return (result_real, result_imag)


def local(
    tokens,
    norm_gain,
    conv_value,
    conv_gate,
    state_feed,
    conv_taps,
    chan_gain,
    chan_shift,
    conv_project,
    decay_rate,
    frequency,
    input_real,
    input_imag,
    output_real,
    output_imag,
    skip_gain,
    state_value,
    state_gate,
    initial_state,
):
    highest = lax.Precision.HIGHEST
    floats = tokens.astype(jnp.float32)
    normed = (
        floats * lax.rsqrt(jnp.mean(floats * floats, axis=1, keepdims=True) + 1e-06) * norm_gain
    ).astype(jnp.bfloat16)
    length = tokens.shape[0]
    width = conv_value.shape[1]
    in_block = jnp.concatenate([conv_value, conv_gate, state_feed], axis=1)
    projected = jnp.dot(
        normed,
        lax.all_gather(in_block, "sp", axis=0, tiled=True),
        preferred_element_type=jnp.float32,
    )
    gated_linear = (projected[:, :width] * jax.nn.sigmoid(projected[:, width : 2 * width])).astype(
        jnp.bfloat16
    )
    state_drive = projected[:, 2 * width :].astype(jnp.bfloat16)
    kernel = conv_taps.shape[0]
    before = passed_along(gated_linear[length - (kernel - 1) :], "sp", 1)
    padded = jnp.concatenate([before, gated_linear], axis=0).astype(jnp.float32)
    conv_sum = jnp.zeros((length, width), jnp.float32)
    for offset in range(kernel):
        conv_sum = conv_sum + conv_taps[offset] * padded[offset : offset + length]
    conv_out = conv_sum.astype(jnp.bfloat16)
    seq_devices = lax.axis_size("sp")
    total_tokens = length * seq_devices
    groups, state_size, group_size = input_real.shape
    flat = groups * state_size
    rate_real = -decay_rate / total_tokens
    magnitude = jnp.exp(rate_real)
    step_real = magnitude * jnp.cos(frequency)
    step_imag = magnitude * jnp.sin(frequency)
    modulus = rate_real * rate_real + frequency * frequency
    lift_real = step_real - 1.0
    factor_real = (lift_real * rate_real + step_imag * frequency) / modulus
    factor_imag = (step_imag * rate_real - lift_real * frequency) / modulus
    drive_real = factor_real[..., None] * input_real - factor_imag[..., None] * input_imag
    drive_imag = factor_real[..., None] * input_imag + factor_imag[..., None] * input_real
    grouped = state_drive.astype(jnp.float32).reshape(length, groups, group_size)
    pushed_real = jnp.einsum("gph,tgh->tgp", drive_real, grouped, precision=highest).reshape(
        length, flat
    )
    pushed_imag = jnp.einsum("gph,tgh->tgp", drive_imag, grouped, precision=highest).reshape(
        length, flat
    )
    base_real = step_real.reshape(flat)
    base_imag = step_imag.reshape(flat)
    square_size = base_real * base_real + base_imag * base_imag
    back_real = base_real / square_size
    back_imag = -base_imag / square_size
    positions = lax.iota(jnp.int32, length)
    counted = positions + 1
    power_real, power_imag = power_table(base_real, base_imag, counted, length)
    undo_real, undo_imag = power_table(back_real, back_imag, counted, length)
    scaled_real, scaled_imag = rotate(undo_real, undo_imag, pushed_real, pushed_imag)
    lower = (positions[:, None] >= positions[None, :]).astype(jnp.float32)
    summed_real = jnp.dot(lower, scaled_real, precision=highest)
    summed_imag = jnp.dot(lower, scaled_imag, precision=highest)
    local_real, local_imag = rotate(power_real, power_imag, summed_real, summed_imag)
    span_real, span_imag = (power_real[-1], power_imag[-1])
    last_real, last_imag = (local_real[-1], local_imag[-1])
    start_real = initial_state[0].reshape(flat)
    start_imag = initial_state[1].reshape(flat)
    finals = lax.all_gather(jnp.stack([last_real, last_imag])[None], "sp", axis=0, tiled=True)
    position = lax.axis_index("sp")
    device_ids = lax.iota(jnp.int32, seq_devices)
    lag = jnp.maximum(position - 1 - device_ids, 0)
    weight_real, weight_imag = power_table(span_real, span_imag, lag, seq_devices)
    before_mask = (device_ids < position).astype(jnp.float32)[:, None]
    moved_real, moved_imag = rotate(weight_real, weight_imag, finals[:, 0], finals[:, 1])
    lead_real, lead_imag = power_table(
        span_real, span_imag, jnp.stack([position, jnp.int32(seq_devices)]), seq_devices
    )
    opening_real, opening_imag = rotate(lead_real[0], lead_imag[0], start_real, start_imag)
    entry_real = opening_real + jnp.sum(moved_real * before_mask, axis=0)
    entry_imag = opening_imag + jnp.sum(moved_imag * before_mask, axis=0)
    tail_real, tail_imag = power_table(
        span_real, span_imag, seq_devices - 1 - device_ids, seq_devices
    )
    carried_real, carried_imag = rotate(tail_real, tail_imag, finals[:, 0], finals[:, 1])
    closing_real, closing_imag = rotate(lead_real[1], lead_imag[1], start_real, start_imag)
    final_real = closing_real + jnp.sum(carried_real, axis=0)
    final_imag = closing_imag + jnp.sum(carried_imag, axis=0)
    final_state = jnp.stack([final_real, final_imag]).reshape(2, groups, state_size)
    state_real = (power_real * entry_real - power_imag * entry_imag + local_real).reshape(
        length, groups, state_size
    )
    state_imag = (power_real * entry_imag + power_imag * entry_real + local_imag).reshape(
        length, groups, state_size
    )
    response = jnp.einsum("ghp,tgp->tgh", output_real, state_real, precision=highest) - jnp.einsum(
        "ghp,tgp->tgh", output_imag, state_imag, precision=highest
    )
    response = response.reshape(length, groups * group_size) + skip_gain * state_drive.astype(
        jnp.float32
    )
    activated = jax.nn.gelu(response).astype(jnp.bfloat16)
    conv_rows, activated_rows = (
        lax.all_gather(conv_out, "tp", axis=1, tiled=True),
        lax.all_gather(activated, "tp", axis=1, tiled=True),
    )
    conv_full = conv_rows.astype(jnp.float32)
    row_mean = jnp.mean(conv_full, axis=1, keepdims=True)
    centred = conv_full - row_mean
    variance = jnp.mean(centred * centred, axis=1, keepdims=True)
    conv_act = jax.nn.silu(centred * lax.rsqrt(variance + 1e-05) * chan_gain + chan_shift).astype(
        jnp.bfloat16
    )
    columns = conv_project.shape[1]
    out_block = jnp.concatenate([conv_project, state_value, state_gate], axis=1)
    piece = lax.all_gather(out_block, "sp", axis=0, tiled=True)
    conv_branch = jnp.dot(conv_act, piece[:, :columns], preferred_element_type=jnp.float32)
    state_both = jnp.dot(activated_rows, piece[:, columns:], preferred_element_type=jnp.float32)
    mixer_out = (
        conv_branch + state_both[:, :columns] * jax.nn.sigmoid(state_both[:, columns:])
    ).astype(jnp.bfloat16)
    return (mixer_out, final_state)


def remote(source, target, send_sem, recv_sem, device):
    return pltpu.make_async_remote_copy(
        src_ref=source,
        dst_ref=target,
        send_sem=send_sem,
        recv_sem=recv_sem,
        device_id=device,
        device_id_type=pl.DeviceIdType.MESH,
    )


def span_of(start, size, unit=None):
    return pl.ds(pl.multiple_of(start, unit or size), size)


class Place:
    def __init__(self):
        outer, self.inner, self.core = (
            lax.axis_index("outer"),
            lax.axis_index("inner"),
            lax.axis_index("tp"),
        )
        self.half = outer // 2
        self.plane = outer % 2
        self.slot = self.plane * 4 + self.inner
        self.here = outer * 4 + self.inner
        self.partner = self.device_of(self.slot, 1 - self.half)
        y, x = (self.inner // 2, self.inner % 2)
        self.members = []
        for flip in range(8):
            plane = 1 - self.plane if flip & 4 else self.plane
            row = 1 - y if flip & 2 else y
            column = 1 - x if flip & 1 else x
            self.members.append(plane * 4 + row * 2 + column)
        flip_x, flip_y = (self.members[1] % 4, self.members[2] % 4)
        first = flip_x * (1 - self.core) + flip_y * self.core
        second = flip_y * (1 - self.core) + flip_x * self.core
        opposite = 3 - self.inner
        near, far = (self.plane * 4, (1 - self.plane) * 4)
        self.order = [
            near + self.inner,
            far + self.inner,
            near + first,
            far + first,
            near + second,
            far + second,
            near + opposite,
            far + opposite,
        ]
        self.lanes = {
            "z": self.device_of(far + self.inner, self.half),
            "first": self.device_of(near + first, self.half),
            "second": self.device_of(near + second, self.half),
            "peer": (outer, self.inner, 1 - self.core),
        }

    def device_of(self, slot, half):
        return (half * 2 + slot // 4, slot % 4, self.core)


class WeightFlow:
    def __init__(self, place, sources, held, sent, got, passed, kept):
        self.place, self.sources, self.held = (place, sources, held)
        self.sent, self.got, self.passed, self.kept = (sent, got, passed, kept)
        self.rows = sources[0].shape[0]
        self.columns = sources[0].shape[1] // 8

    def piece(self, index):
        return self.held.at[span_of(index * self.rows, self.rows)]

    def part(self, which):
        rows = span_of(self.place.here * self.rows, self.rows)
        return self.held.at[rows, pl.ds(which * self.columns, self.columns)]

    def origin(self, which, slot):
        return self.sources[which].at[:, span_of(slot * self.columns, self.columns)]

    def keep(self, which):
        place = self.place
        return pltpu.make_async_copy(
            self.origin(which, place.slot), self.part(which), self.kept.at[which]
        )

    def near(self, flip, which):
        place = self.place
        slot = place.members[flip]
        return remote(
            self.origin(which, slot),
            self.part(which),
            self.sent.at[flip - 1],
            self.got.at[place.here],
            place.device_of(slot, place.half),
        )

    def whole(self, index, flip, device):
        piece = self.piece(index)
        return remote(piece, piece, self.passed.at[flip], self.got.at[index], device)

    def near_index(self, flip):
        return self.place.half * 8 + self.place.members[flip]

    def far_index(self, flip):
        return (1 - self.place.half) * 8 + self.place.members[flip]

    def start(self):
        for which in range(3):
            self.keep(which).start()
        for flip in range(1, 8):
            for which in range(3):
                self.near(flip, which).start()

    def relay(self, flip):
        passing = self.whole(self.near_index(flip), flip, self.place.partner)
        if flip == 0:
            for which in range(3):
                self.keep(which).wait()
        else:
            passing.wait_recv()
        passing.start()

    def far_wait(self, flip):
        self.whole(self.far_index(flip), flip, self.place.partner).wait_recv()

    def drain(self):
        place = self.place
        for flip in range(1, 8):
            piece = self.piece(place.here)
            device = place.device_of(place.members[flip], place.half)
            remote(
                piece, piece, self.sent.at[flip - 1], self.got.at[place.here], device
            ).wait_send()
        for flip in range(8):
            self.whole(self.near_index(flip), flip, place.partner).wait_send()


LANES = (
    ("z", "first", "second", "peer"),
    ("first", "second", "peer"),
    ("second", "peer"),
    ("second", "peer"),
    ("peer",),
    ("peer",),
    ("peer",),
    ("peer",),
)


class GatherFlow:
    def __init__(self, place, view, parts, sent, got, own_lanes=4):
        self.place, self.view, self.parts, self.sent, self.got = (place, view, parts, sent, got)
        self.own_lanes = own_lanes

    def copy(self, block, part, lane):
        core = self.place.core
        origin = self.place.order[block]
        piece = self.view(origin, part, core)
        names = LANES[block]
        number = sum(len(names) for names in LANES[:block]) + names.index(lane)
        return remote(
            piece,
            piece,
            self.sent.at[part, number],
            self.got.at[origin, core * self.parts + part],
            self.place.lanes[lane],
        )

    def lanes_of(self, block):
        return LANES[0][: self.own_lanes] if block == 0 else LANES[block]

    def send(self, block, part):
        for lane in self.lanes_of(block):
            self.copy(block, part, lane).start()

    def relay(self, block, part):
        self.copy(block, part, LANES[block][0]).wait_recv()
        self.send(block, part)

    def peer_wait(self, block, part):
        side = 1 - self.place.core
        origin = self.place.order[block]
        piece = self.view(origin, part, side)
        remote(
            piece,
            piece,
            self.sent.at[part, 0],
            self.got.at[origin, side * self.parts + part],
            self.place.lanes["peer"],
        ).wait_recv()

    def drain(self):
        for part in range(self.parts):
            for block in range(8):
                for lane in self.lanes_of(block):
                    self.copy(block, part, lane).wait_send()


def dot(left, right):
    return jnp.dot(left, right, preferred_element_type=jnp.float32)


def dot_rows(left, right):
    return lax.dot_general(
        left, right, (((1,), (1,)), ((), ())), preferred_element_type=jnp.float32
    )


def halves(value):
    high = value.astype(jnp.bfloat16)
    return (high, (value - high.astype(jnp.float32)).astype(jnp.bfloat16))


def build_matrices(groups, chunk, small_ref, vec_ref, skip_ref, push, emit, inside, span, drive):
    width = small_ref.shape[0] // 4
    flat = small_ref.shape[1]
    lanes = groups * width
    row_group = lax.broadcasted_iota(jnp.int32, (lanes, flat), 0) // width
    column_group = lax.broadcasted_iota(jnp.int32, (lanes, flat), 1) // (flat // groups)
    mask = (row_group == column_group).astype(jnp.float32)

    def spread(which):
        return jnp.concatenate([small_ref[which * width : (which + 1) * width]] * groups, 0) * mask

    step_real, step_imag = (vec_ref[0:1], vec_ref[1:2])
    powers = [(jnp.ones_like(step_real), jnp.zeros_like(step_real))]
    for _ in range(chunk):
        powers.append(rotate(*powers[-1], step_real, step_imag))
    span[0:1] = powers[chunk][0]
    span[1:2] = powers[chunk][1]
    drive_real, drive_imag = (spread(0), spread(1))
    for place in range(chunk):
        rows = pl.ds(place * lanes, lanes)
        for side, value in enumerate(rotate(*powers[chunk - 1 - place], drive_real, drive_imag)):
            for part, piece in enumerate(halves(value)):
                push[part, rows, pl.ds(side * flat, flat)] = piece
    for side, value in enumerate((drive_real, drive_imag)):
        for part, piece in enumerate(halves(value)):
            drive[part, :, pl.ds(side * flat, flat)] = piece
    out_real, out_imag = (spread(2), spread(3))
    inside[...] = jnp.zeros_like(inside)
    diagonal = lax.broadcasted_iota(jnp.int32, (lanes, lanes), 0) == lax.broadcasted_iota(
        jnp.int32, (lanes, lanes), 1
    )
    for lag in range(chunk + 1):
        real, imag = rotate(*powers[lag], out_real, out_imag)
        response = jnp.zeros((lanes, lanes), jnp.float32)
        for side, value in enumerate((real, -imag)):
            columns = pl.ds(side * flat, flat)
            high, low = halves(value)
            if lag > 0:
                rows = pl.ds((lag - 1) * lanes, lanes)
                emit[0, rows, columns] = high
                emit[1, rows, columns] = low
            if lag < chunk:
                response = response + dot_rows(drive[0, :, columns], high)
                response = response + dot_rows(drive[1, :, columns], high)
                response = response + dot_rows(drive[0, :, columns], low)
        if lag < chunk:
            if lag == 0:
                response = response + jnp.where(diagonal, skip_ref[...], 0.0)
            high, low = halves(response)
            for place in range(chunk - lag):
                rows, columns = (pl.ds(place * lanes, lanes), pl.ds((place + lag) * lanes, lanes))
                inside[0, rows, columns] = high
                inside[1, rows, columns] = low


def mixer_kernel(
    groups,
    chunk,
    token_ref,
    value_ref,
    gate_ref,
    feed_ref,
    project_ref,
    svalue_ref,
    sgate_ref,
    gain_ref,
    small_ref,
    vec_ref,
    taps_ref,
    skip_ref,
    chan_gain_ref,
    chan_shift_ref,
    out_ref,
    final_ref,
    raw,
    normed,
    w_in,
    total,
    w_out,
    both,
    acted,
    mixed,
    gated,
    feed,
    answer,
    rows_in,
    pushed,
    entry,
    push,
    emit,
    inside,
    drive,
    span,
    last,
    start,
    in_sent,
    in_got,
    in_passed,
    out_sent,
    out_got,
    out_passed,
    kept,
    token_sent,
    token_got,
    both_sent,
    both_got,
    mix_sent,
    mix_got,
    final_sent,
    final_got,
    edge,
    single,
):
    place = Place()
    half, slot, core = (place.half, place.slot, place.core)
    length, model = raw.shape
    tokens = normed.shape[0]
    side = model // 2
    share = feed.shape[1]
    wide = both.shape[2]
    token_parts, both_parts = (token_sent.shape[0], both_sent.shape[0])
    token_rows, both_rows = (length // token_parts, tokens // both_parts)

    def token_view(origin, part, which):
        rows = span_of(origin * length + part * token_rows, token_rows, 16)
        return normed.at[rows, span_of(which * side, side)]

    def both_view(origin, part, which):
        columns = span_of((which * 8 + origin) * share, share)
        return both.at[:, pl.ds(part * both_rows, both_rows), columns]

    inward = WeightFlow(
        place, (value_ref, gate_ref, feed_ref), w_in, in_sent, in_got, in_passed, kept.at[0]
    )
    outward = WeightFlow(
        place, (project_ref, svalue_ref, sgate_ref), w_out, out_sent, out_got, out_passed, kept.at[1]
    )
    token_flow = GatherFlow(place, token_view, token_parts, token_sent, token_got, 3)
    both_flow = GatherFlow(place, both_view, both_parts, both_sent, both_got)

    load = pltpu.make_async_copy(token_ref, raw, single.at[0])
    load.start()
    inward.start()
    load.wait()
    gain = gain_ref[...]
    for part in range(token_parts):

        def norm(step, _):
            floats = raw[span_of(part * token_rows + step * 16, 16)].astype(jnp.float32)
            scale = lax.rsqrt(jnp.mean(floats * floats, axis=1, keepdims=True) + 1e-06)
            rows = span_of(slot * length + part * token_rows + step * 16, 16)
            normed[rows] = (floats * scale * gain).astype(jnp.bfloat16)
            return 0

        lax.fori_loop(0, token_rows // 16, norm, 0)
        token_flow.send(0, part)
    for flip in range(8):
        inward.relay(flip)
    build_matrices(
        groups, chunk, small_ref, vec_ref, skip_ref, push, emit, inside, span, drive
    )
    for part in range(token_parts):
        token_flow.relay(1, part)
        token_flow.relay(2, part)
    for part in range(token_parts):
        token_flow.relay(3, part)
    outward.start()
    for part in range(token_parts):
        for block in range(4, 8):
            token_flow.relay(block, part)
    outward.relay(0)
    for part in range(token_parts):
        for block in range(1, 8):
            token_flow.peer_wait(block, part)

    block_rows = 256

    def first_product(step, _):
        rows = span_of(step * block_rows, block_rows)
        depth = span_of(half * side, side)
        total[rows] = dot(normed[rows, depth], w_in[depth])
        return 0

    lax.fori_loop(0, tokens // block_rows, first_product, 0)
    depth_size = 2 * inward.rows
    for flip in range(0, 8, 2):
        inward.far_wait(flip)
        inward.far_wait(flip + 1)
        pair = inward.far_index(flip) // 2

        def add_product(step, _):
            rows = span_of(step * block_rows, block_rows)
            depth = span_of(pair * depth_size, depth_size)
            total[rows] = total[rows] + dot(normed[rows, depth], w_in[depth])
            return 0

        lax.fori_loop(0, tokens // block_rows, add_product, 0)

    margin = gated.shape[0] - tokens
    gated_edge = remote(
        gated.at[pl.ds(tokens, margin)],
        gated.at[pl.ds(0, margin)],
        edge.at[0],
        edge.at[1],
        place.partner,
    )
    state_edge = remote(last, start, edge.at[2], edge.at[3], place.partner)

    def gate(step, _):
        rows = span_of(step * block_rows, block_rows)
        value = total[rows]
        product = value[:, :share] * jax.nn.sigmoid(value[:, share : 2 * share])
        gated[span_of(margin + step * block_rows, block_rows, 8)] = product.astype(
            jnp.bfloat16
        ).astype(jnp.float32)
        feed[rows] = value[:, 2 * share :].astype(jnp.bfloat16).astype(jnp.float32)
        return 0

    lax.fori_loop(0, tokens // block_rows, gate, 0)

    @pl.when(half == 0)
    def _():
        gated_edge.start()
        gated[0:margin] = jnp.zeros((margin, share), jnp.float32)

    count = tokens // chunk
    for offset in range(chunk):
        rows_in[:, offset * share : (offset + 1) * share] = feed[
            pl.ds(offset, count, stride=chunk), :
        ].astype(jnp.bfloat16)
    block_columns = 256

    def push_product(step, _):
        columns = span_of(step * block_columns, block_columns)
        left = rows_in[...]
        pushed[:, columns] = dot(left, push[0, :, columns]) + dot(left, push[1, :, columns])
        return 0

    lax.fori_loop(0, pushed.shape[1] // block_columns, push_product, 0)
    flat = pushed.shape[1] // 2

    def scan(real, imag):
        span_real, span_imag = (span[0:1], span[1:2])

        def advance(step, carried):
            real, imag = carried
            for offset in range(8):
                index = pl.ds(step * 8 + offset, 1)
                entry[index, pl.ds(0, flat)] = real
                entry[index, pl.ds(flat, flat)] = imag
                next_real, next_imag = rotate(span_real, span_imag, real, imag)
                real = next_real + pushed[index, pl.ds(0, flat)]
                imag = next_imag + pushed[index, pl.ds(flat, flat)]
            return (real, imag)

        real, imag = lax.fori_loop(0, count // 8, advance, (real, imag))
        for row in range(flat // 128):
            last[row : row + 1] = real[:, row * 128 : (row + 1) * 128]
            last[flat // 128 + row : flat // 128 + row + 1] = imag[:, row * 128 : (row + 1) * 128]

    @pl.when(half == 0)
    def _():
        scan(vec_ref[2:3], vec_ref[3:4])
        state_edge.start()

    @pl.when(half == 1)
    def _():
        gated_edge.wait_recv()

    own_columns = span_of((core * 8 + slot) * share, share)
    kernel = taps_ref.shape[0]
    conv_rows = 64
    ahead = margin - (kernel - 1)

    def convolve(step, _):
        window = gated[span_of(step * conv_rows, conv_rows + margin, 8)]
        summed = jnp.zeros((conv_rows, share), jnp.float32)
        for residue in range(8):
            shifted = window[residue : residue + conv_rows + margin - 8] if residue else window
            for tap in range(kernel):
                if (ahead + tap) % 8 == residue:
                    begin = ahead + tap - residue
                    summed = summed + taps_ref[tap : tap + 1] * shifted[begin : begin + conv_rows]
        both[0, span_of(step * conv_rows, conv_rows), own_columns] = summed.astype(jnp.bfloat16)
        return 0

    lax.fori_loop(0, tokens // conv_rows, convolve, 0)

    def final_copy(slot_to, half_to, number):
        return remote(
            last,
            final_ref.at[slot],
            final_sent.at[number],
            final_got.at[slot],
            place.device_of(slot_to, half_to),
        )

    final_keep = pltpu.make_async_copy(last, final_ref.at[slot], single.at[1])

    def final_copies():
        for flip in range(1, 8):
            yield final_copy(place.members[flip], 1, flip)
        for flip in range(8):
            yield final_copy(place.members[flip], 0, 8 + flip)

    @pl.when(half == 1)
    def _():
        state_edge.wait_recv()
        rows = flat // 128
        scan(
            jnp.concatenate([start[row : row + 1] for row in range(rows)], axis=1),
            jnp.concatenate([start[rows + row : rows + row + 1] for row in range(rows)], axis=1),
        )
        final_keep.start()

    for pair in range(chunk // 2):
        columns = pl.ds(pair * 2 * share, 2 * share)
        before = (pair + 1) * 2 * share
        left = rows_in[:, :before]
        response = dot(left, inside[0, :before, columns]) + dot(left, inside[1, :before, columns])
        high, low = halves(entry[...])
        response = response + dot_rows(high, emit[0, columns]) + dot_rows(low, emit[0, columns])
        response = response + dot_rows(high, emit[1, columns])
        active = jax.nn.gelu(response)
        for offset in range(2):
            answer[pl.ds(2 * pair + offset, count, stride=chunk), :] = active[
                :, offset * share : (offset + 1) * share
            ]

    def store_answer(step, _):
        rows = span_of(step * block_rows, block_rows)
        both[1, rows, own_columns] = answer[rows].astype(jnp.bfloat16)
        return 0

    lax.fori_loop(0, tokens // block_rows, store_answer, 0)
    for part in range(both_parts):
        both_flow.send(0, part)

    @pl.when(half == 1)
    def _():
        for copy in final_copies():
            copy.start()

    for flip in range(1, 8):
        outward.relay(flip)
    for part in range(both_parts):
        both_flow.relay(1, part)
        both_flow.relay(2, part)
    for part in range(both_parts):
        both_flow.relay(3, part)
    for flip in range(8):
        outward.far_wait(flip)

    output = w_out.shape[1] // 3
    finish_rows = 128

    def mix_copy(member):
        return remote(
            mixed.at[pl.ds(member * length, length)],
            out_ref.at[:, span_of(slot * output, output)],
            mix_sent.at[member],
            mix_got.at[slot],
            place.device_of(member, half),
        )

    def mix_keep(member):
        return pltpu.make_async_copy(
            mixed.at[pl.ds(member * length, length)],
            out_ref.at[:, span_of(slot * output, output)],
            mix_sent.at[member],
        )

    for part in range(both_parts):
        for block in range(4, 8):
            both_flow.relay(block, part)
        for block in range(8):
            both_flow.peer_wait(block, part)

        def activate(step, _):
            rows = span_of(step * 16, 16)
            full = both[0, span_of(part * both_rows + step * 16, 16)].astype(jnp.float32)
            centred = full - jnp.mean(full, axis=1, keepdims=True)
            variance = jnp.mean(centred * centred, axis=1, keepdims=True)
            value = centred * lax.rsqrt(variance + 1e-05) * chan_gain_ref[...] + chan_shift_ref[...]
            acted[rows] = jax.nn.silu(value).astype(jnp.bfloat16)
            return 0

        lax.fori_loop(0, both_rows // 16, activate, 0)

        def finish(step, _):
            local_rows = span_of(step * finish_rows, finish_rows)
            rows = span_of(part * both_rows + step * finish_rows, finish_rows)
            branch = dot(acted[local_rows], w_out[:, :output])
            state = dot(both[1, rows], w_out[:, output:])
            mixed[rows] = (
                branch + state[:, :output] * jax.nn.sigmoid(state[:, output:])
            ).astype(jnp.bfloat16)
            return 0

        lax.fori_loop(0, both_rows // finish_rows, finish, 0)
        for member in range(part * both_rows // length, (part + 1) * both_rows // length):

            @pl.when(slot == member)
            def _():
                mix_keep(member).start()

            @pl.when(slot != member)
            def _():
                mix_copy(member).start()

    inward.drain()
    outward.drain()
    token_flow.drain()
    both_flow.drain()

    @pl.when(half == 0)
    def _():
        gated_edge.wait_send()
        state_edge.wait_send()

    for flip in range(8):
        origin = place.members[flip]
        arrival = remote(
            last, final_ref.at[origin], final_sent.at[0], final_got.at[origin], place.partner
        )
        if flip == 0:
            pl.when(half == 0)(arrival.wait_recv)
        else:
            arrival.wait_recv()

    @pl.when(half == 1)
    def _():
        final_keep.wait()
        for copy in final_copies():
            copy.wait_send()

    for member in range(8):

        @pl.when(slot == member)
        def _():
            mix_keep(member).wait()

        @pl.when(slot != member)
        def _():
            mix_copy(member).wait_send()

    for flip in range(1, 8):
        origin = place.members[flip]
        remote(
            mixed.at[pl.ds(0, length)],
            out_ref.at[:, span_of(origin * output, output)],
            mix_sent.at[0],
            mix_got.at[origin],
            place.partner,
        ).wait_recv()


def cube_local(
    tokens,
    norm_gain,
    conv_value,
    conv_gate,
    state_feed,
    conv_taps,
    chan_gain,
    chan_shift,
    conv_project,
    decay_rate,
    frequency,
    input_real,
    input_imag,
    output_real,
    output_imag,
    skip_gain,
    state_value,
    state_gate,
    initial_state,
):
    outer, inner = (lax.axis_size("outer"), lax.axis_size("inner"))
    devices = outer * inner
    slot = lax.axis_index("outer") % 2 * inner + lax.axis_index("inner")
    length, model = tokens.shape
    span = length * devices // 2
    wide = chan_gain.shape[0]
    share = conv_value.shape[1] // 8
    output = conv_project.shape[1] // 8
    groups, states, width = input_real.shape
    groups //= 8
    flat = groups * states
    chunk = 8

    def own(value, size, axis=0):
        return lax.dynamic_slice_in_dim(value, slot * size, size, axis=axis)

    rate_real = -own(decay_rate, groups) / (length * devices)
    turn = own(frequency, groups)
    magnitude = jnp.exp(rate_real)
    step_real = magnitude * jnp.cos(turn)
    step_imag = magnitude * jnp.sin(turn)
    modulus = rate_real * rate_real + turn * turn
    lift_real = step_real - 1.0
    factor_real = (lift_real * rate_real + step_imag * turn) / modulus
    factor_imag = (step_imag * rate_real - lift_real * turn) / modulus
    in_real, in_imag = (own(input_real, groups), own(input_imag, groups))
    drive_real = factor_real[..., None] * in_real - factor_imag[..., None] * in_imag
    drive_imag = factor_real[..., None] * in_imag + factor_imag[..., None] * in_real
    small = jnp.concatenate(
        [value.transpose(2, 0, 1).reshape(width, flat) for value in (drive_real, drive_imag)]
        + [
            own(value, groups).transpose(1, 0, 2).reshape(width, flat)
            for value in (output_real, output_imag)
        ],
        axis=0,
    )
    begin = own(initial_state, groups, 1)
    vec = jnp.stack([step_real, step_imag, begin[0], begin[1]]).reshape(4, flat)
    vmem = functools.partial(pltpu.VMEM)
    dma = pltpu.SemaphoreType.DMA
    half_word, word = (jnp.bfloat16, jnp.float32)
    margin = 32
    token_parts, both_parts = (2, 4)
    count = span // chunk
    any_spec = pl.BlockSpec(memory_space=pl.ANY)
    near_spec = pl.BlockSpec(memory_space=pltpu.VMEM)
    mixer_out, final = pl.pallas_call(
        functools.partial(mixer_kernel, groups, chunk),
        out_shape=(
            jax.ShapeDtypeStruct((length, 8 * output), half_word),
            jax.ShapeDtypeStruct((8, 2 * flat // 128, 128), word),
        ),
        in_specs=[any_spec] * 7 + [near_spec] * 7,
        out_specs=(any_spec, any_spec),
        scratch_shapes=[
            vmem((length, model), half_word),
            vmem((span, model), half_word),
            vmem((devices * conv_value.shape[0], 3 * share), half_word),
            vmem((span, 3 * share), word),
            vmem((devices * conv_project.shape[0], 3 * output), half_word),
            vmem((2, span, wide), half_word),
            vmem((span // both_parts, wide), half_word),
            vmem((span, output), half_word),
            vmem((margin + span, share), word),
            vmem((span, share), word),
            vmem((span, share), word),
            vmem((count, chunk * share), half_word),
            vmem((count, 2 * flat), word),
            vmem((count, 2 * flat), word),
            vmem((2, chunk * share, 2 * flat), half_word),
            vmem((2, chunk * share, 2 * flat), half_word),
            vmem((2, chunk * share, chunk * share), half_word),
            vmem((2, share, 2 * flat), half_word),
            vmem((2, flat), word),
            vmem((2 * flat // 128, 128), word),
            vmem((2 * flat // 128, 128), word),
            dma((7,)),
            dma((16,)),
            dma((8,)),
            dma((7,)),
            dma((16,)),
            dma((8,)),
            dma((2, 3)),
            dma((token_parts, 15)),
            dma((8, 2 * token_parts)),
            dma((both_parts, 15)),
            dma((8, 2 * both_parts)),
            dma((8,)),
            dma((8,)),
            dma((16,)),
            dma((8,)),
            dma((4,)),
            dma((2,)),
        ],
        compiler_params=pltpu.CompilerParams(
            has_side_effects=True, vmem_limit_bytes=67043328
        ),
    )(
        tokens,
        conv_value,
        conv_gate,
        state_feed,
        conv_project,
        state_value,
        state_gate,
        norm_gain[None],
        small,
        vec,
        own(conv_taps, share, 1),
        own(skip_gain, share)[None],
        chan_gain[None],
        chan_shift[None],
    )
    final_state = final.reshape(8, 2, groups, states).transpose(1, 0, 2, 3)
    return (mixer_out, final_state.reshape(2, 8 * groups, states))


def specs_of(seq):
    in_specs = (
        P(seq, None),
        P(),
        P(seq, "tp"),
        P(seq, "tp"),
        P(seq, "tp"),
        P(None, "tp"),
        P(),
        P(),
        P(seq, "tp"),
        P("tp", None),
        P("tp", None),
        P("tp", None, None),
        P("tp", None, None),
        P("tp", None, None),
        P("tp", None, None),
        P("tp"),
        P(seq, "tp"),
        P(seq, "tp"),
        P(None, "tp", None),
    )
    return (in_specs, (P(seq, "tp"), P(None, "tp", None)))


def solution(mesh):
    seq_devices, cores = (mesh.shape["sp"], mesh.shape["tp"])
    fine = jax.sharding.Mesh(
        mesh.devices.reshape(seq_devices // 4, 4, cores), ("outer", "inner", "tp")
    )

    def run(*args):
        groups = args[9].shape[0]
        if cores == 2 and seq_devices == 16 and groups % (cores * 8) == 0:
            in_specs, out_specs = specs_of(("outer", "inner"))
            body = jax.shard_map(
                cube_local, mesh=fine, in_specs=in_specs, out_specs=out_specs, check_vma=False
            )
        else:
            in_specs, out_specs = specs_of("sp")
            body = jax.shard_map(
                local, mesh=mesh, in_specs=in_specs, out_specs=out_specs, check_vma=False
            )
        return body(*args)

    return run
```

time: 370 us -> 262 us (0.71)
  matrix products: 34.9 us -> 0 us
  local copies, waits for them, and re-layouts: 37.4 us -> 8.43 us
  other arithmetic: 27.8 us -> 2.91 us
  between operations: 15.5 us -> 0.7 us
  Pallas kernels: 236 us -> 249 us
  waiting for transfers between devices: 10.9 us -> 0 us
  starting transfers between devices: 6.81 us -> 0 us
    dot_general x8 -> x0, matrix products: 34.9 us -> none  [the longest x1 10.2 us: channel_local(): lax.dot_general(in_block, all_half, (((1,), (1,)), ((), ())), preferred_e...]
    pallas_call x3 -> x1, Pallas kernels: 236 us -> 249 us  [cube_local(): pl.pallas_call(functools.partial(mixer_kernel, groups, chunk), out_shape=...]
    convert_element_type x8 -> x0, other arithmetic: 11.5 us -> none  [the longest x1 7.35 us: channel_local(): conv_out = conv_sum.astype(jnp.bfloat16)]
    mul x13 -> x0, local copies, waits for them, and re-layouts: 10.9 us -> none  [the longest x8 6.62 us: block_diagonal(): blocks[:, :, :, None, :]]
    all_to_all x1 -> x0, waiting for transfers between devices: 10.9 us -> none  [channel_local(): mixer = lax.all_to_all(mixer, 'inner', 0, 0, tiled=True)]
    transpose x7 -> x5, local copies, waits for them, and re-layouts: 7.14 us -> 0.98 us  [the longest x3 0.93 us: cube_local(): own(value, groups).transpose(1, 0, 2).reshape(width, flat)]
  transfers between devices with their start and end apart: 4 -> 0, of which waited for: 1 -> 0; matrix products, arithmetic and copies ran while one was open for 16% -> 0% of each run, Pallas kernels for 24% -> 0%
where the time goes in v1:
time: 262 us; the launch traced here: 261 us
  Pallas kernels  249 us (95%)
  local copies, waits for them, and re-layouts  8.43 us (3%)
  other arithmetic  2.91 us (1%)
    pallas_call x1, Pallas kernels, cube_local(): pl.pallas_call(functools.partial(mixer_kernel, groups, chunk), out_shape=...  249 us

profile of v1, /device:TPU:0, one launch (start us, length us, event | category | flops | bytes accessed | tf_op | source)
XLA Modules:
  0.0 260.9 jit_solution(13593092153225175093)
XLA Ops:
  0.7 1.3 dynamic-slice_bitcast_fusion.2.skip_ref
  2.0 0.7 constant_dynamic-slice_fusion.1
  2.7 0.1 stack.14
  2.8 1.3 constant_dynamic-slice_fusion.taps_ref
  4.1 0.7 cosine_multiply_fusion
  4.8 0.1 stack.12
  4.9 0.1 stack.13
  5.0 0.6 pad_maximum_fusion.1.vec_ref
  5.6 0.9 subtract_bitcast_fusion
  6.5 0.1 reshape.30
  6.6 0.1 reshape.31
  6.7 0.9 dynamic-slice_bitcast_fusion
  7.6 0.1 reshape.33
  7.7 0.1 reshape.32
  7.8 0.7 pad_maximum_fusion.small_ref
  8.5 248.9 %shard_map.194 = (bf16[192,2048]{1,0:T(8,128)(2,1)}, f32[8,8,128]{2,1,0:T(8,128)}) custom-call(bf16[192,4096]{1,0:T(8,128)(2,1)} %token_ref.1, bf16[256,1024]{1,0:T(8,128)(2,1)} %value_ref.1, bf16[256,1024]{1,0:T(8,128)(2,1)} %gate_ref.1, bf16[256,1024]{1,0:T(8,128)(2,1)} %feed_ref.1, bf16[128,2048]{1,0:T(8,128)(2,1)} %project_ref.1, ...), custom_call_target="tpu_custom_call" | custom-call | tf_op jit(solution)/shard_map/pallas_call | solution.py:911
  257.4 0.8 reshape.34
  258.2 0.6 copy_bitcast_fusion
  258.8 2.1 copy.28
  (4 shorter events, 0.1 us)

commit v2 on v1

--- a/solution.py
+++ b/solution.py
@@ -200,6 +200,8 @@
         self.slot = self.plane * 4 + self.inner
         self.here = outer * 4 + self.inner
         self.partner = self.device_of(self.slot, 1 - self.half)
+        self.across = (3 - outer, self.inner, self.core)
+        self.inside = jnp.logical_or(outer == 1, outer == 2)
         y, x = (self.inner // 2, self.inner % 2)
         self.members = []
         for flip in range(8):
@@ -234,78 +236,144 @@
 
 
 class WeightFlow:
-    def __init__(self, place, sources, held, sent, got, passed, kept):
-        self.place, self.sources, self.held = (place, sources, held)
-        self.sent, self.got, self.passed, self.kept = (sent, got, passed, kept)
+    def __init__(self, place, sources, held, stage, sent, got, staged, kept):
+        self.place, self.sources, self.held, self.stage = (place, sources, held, stage)
+        self.sent, self.got, self.staged, self.kept = (sent, got, staged, kept)
         self.rows = sources[0].shape[0]
         self.columns = sources[0].shape[1] // 8
+        self.peers = [place.members[flip] % 4 for flip in range(4)]
 
     def piece(self, index):
         return self.held.at[span_of(index * self.rows, self.rows)]
 
-    def part(self, which):
-        rows = span_of(self.place.here * self.rows, self.rows)
-        return self.held.at[rows, pl.ds(which * self.columns, self.columns)]
-
-    def origin(self, which, slot):
+    def part(self, other, which):
+        columns = pl.ds(which * self.columns, self.columns)
+        if other:
+            return self.stage.at[self.place.inner, :, columns]
+        return self.held.at[span_of(self.place.here * self.rows, self.rows), columns]
+
+    def origin(self, other, which, peer):
+        plane = 1 - self.place.plane if other else self.place.plane
+        slot = plane * 4 + peer
         return self.sources[which].at[:, span_of(slot * self.columns, self.columns)]
 
-    def keep(self, which):
+    def keep(self, other, which):
+        return pltpu.make_async_copy(
+            self.origin(other, which, self.place.inner),
+            self.part(other, which),
+            self.kept.at[other, which],
+        )
+
+    def near(self, other, flip, which):
         place = self.place
-        return pltpu.make_async_copy(
-            self.origin(which, place.slot), self.part(which), self.kept.at[which]
+        return remote(
+            self.origin(other, which, self.peers[flip]),
+            self.part(other, which),
+            self.sent.at[other, flip],
+            self.staged.at[place.inner] if other else self.got.at[place.here],
+            place.device_of(place.members[flip], place.half),
         )
 
-    def near(self, flip, which):
+    def index(self, flip, half=None, plane=None):
+        half = self.place.half if half is None else half
+        plane = self.place.plane if plane is None else plane
+        return half * 8 + plane * 4 + self.peers[flip]
+
+    def whole(self, index, lane, flip, device, source=None):
+        piece = self.piece(index)
+        return remote(
+            piece if source is None else source,
+            piece,
+            self.sent.at[lane, flip],
+            self.got.at[index],
+            device,
+        )
+
+    def passing(self, kind, flip):
         place = self.place
-        slot = place.members[flip]
-        return remote(
-            self.origin(which, slot),
-            self.part(which),
-            self.sent.at[flip - 1],
-            self.got.at[place.here],
-            place.device_of(slot, place.half),
-        )
-
-    def whole(self, index, flip, device):
-        piece = self.piece(index)
-        return remote(piece, piece, self.passed.at[flip], self.got.at[index], device)
-
-    def near_index(self, flip):
-        return self.place.half * 8 + self.place.members[flip]
-
-    def far_index(self, flip):
-        return (1 - self.place.half) * 8 + self.place.members[flip]
-
-    def start(self):
-        for which in range(3):
-            self.keep(which).start()
-        for flip in range(1, 8):
+        if kind == 0:
+            return self.whole(self.index(flip), 2, flip, place.partner)
+        if kind == 2:
+            index = self.index(flip, plane=1 - place.plane)
+            return self.whole(index, 5, flip, place.partner)
+        index, source = (self.index(flip), self.stage.at[self.peers[flip]])
+        return self.whole(index, 3, flip, place.lanes["z"], source)
+
+    def across(self, flip):
+        source = self.stage.at[self.peers[flip]]
+        return self.whole(self.index(flip), 4, flip, self.place.across, source)
+
+    def hold(self):
+        for other in range(2):
             for which in range(3):
-                self.near(flip, which).start()
-
-    def relay(self, flip):
-        passing = self.whole(self.near_index(flip), flip, self.place.partner)
+                self.keep(other, which).start()
+
+    def start(self, flips):
+        for flip in flips:
+            for other in (1, 0):
+                for which in range(3):
+                    self.near(other, flip, which).start()
+
+    def relay(self, kind, flip):
+        place = self.place
+        passing = self.passing(kind, flip)
+        if kind == 2:
+
+            @pl.when(place.inside)
+            def _():
+                passing.wait_recv()
+                passing.start()
+
+            return
         if flip == 0:
             for which in range(3):
-                self.keep(which).wait()
+                self.keep(kind, which).wait()
+        elif kind == 0:
+            passing.wait_recv()
         else:
-            passing.wait_recv()
+            stage = self.stage.at[self.peers[flip]]
+            remote(
+                stage, stage, self.sent.at[3, flip], self.staged.at[self.peers[flip]], place.partner
+            ).wait_recv()
+        if kind == 1:
+
+            @pl.when(place.inside)
+            def _():
+                self.across(flip).start()
+
         passing.start()
 
-    def far_wait(self, flip):
-        self.whole(self.far_index(flip), flip, self.place.partner).wait_recv()
+    def near_wait(self):
+        @pl.when(jnp.logical_not(self.place.inside))
+        def _():
+            for flip in range(4):
+                self.passing(2, flip).wait_recv()
+
+    def far_wait(self, other, flip):
+        place = self.place
+        plane = 1 - place.plane if other else place.plane
+        index = self.index(flip, 1 - place.half, plane)
+        self.whole(index, 2, flip, place.partner).wait_recv()
+        return index
 
     def drain(self):
         place = self.place
-        for flip in range(1, 8):
+        for flip in range(1, 4):
+            device = place.device_of(place.members[flip], place.half)
             piece = self.piece(place.here)
-            device = place.device_of(place.members[flip], place.half)
-            remote(
-                piece, piece, self.sent.at[flip - 1], self.got.at[place.here], device
-            ).wait_send()
-        for flip in range(8):
-            self.whole(self.near_index(flip), flip, place.partner).wait_send()
+            for other in range(2):
+                remote(
+                    piece, piece, self.sent.at[other, flip], self.got.at[place.here], device
+                ).wait_send()
+        for flip in range(4):
+            self.passing(0, flip).wait_send()
+            self.passing(1, flip).wait_send()
+
+        @pl.when(place.inside)
+        def _():
+            for flip in range(4):
+                self.across(flip).wait_send()
+                self.passing(2, flip).wait_send()
 
 
 LANES = (
@@ -439,6 +507,43 @@
                 inside[1, rows, columns] = low
 
 
+ORDER_A = (
+    "i11", "i01", "i12", "i02", "r10", "r20", "i13", "i03", "r11", "r21", "r30", "w00", "i20",
+    "r12", "r22", "r31", "r40", "i21", "i22", "r13", "r23", "r32", "r41", "i23", "w10", "r33",
+    "s13", "r42", "w11", "w20", "w21", "w32", "r43", "w33",
+)
+ORDER_M = (
+    "o10", "o00",
+)
+ORDER_N = (
+    "o11", "o12", "o01",
+)
+ORDER_B = (
+    "r10", "r20", "r11", "r21", "o13", "r12", "r22", "o02", "r13", "r23", "o03", "r30", "r31",
+    "r14", "r24", "o20", "r32", "r33", "r15", "r25", "o21", "r16", "r26", "r17", "r27", "o22",
+    "o23", "r40", "w20", "w00", "r34", "r41", "w01", "r35", "r42", "w02", "r36", "r43", "w03",
+    "r37", "r44", "w10", "r45", "w11", "r46", "w12", "r47", "w13",
+)
+
+
+def run_order(order, inward, outward, flow, work):
+    for step in order:
+        kind, block, part = (step[0], int(step[1]), int(step[2]))
+        if kind == "i":
+            inward.relay(block, part)
+        elif kind == "o":
+            outward.relay(block, part)
+        elif kind == "s":
+            outward.start(range(block, part + 1))
+        elif kind == "w":
+            work[block](part)
+        elif block == 4:
+            for late in range(4, 8):
+                flow.relay(late, part)
+        else:
+            flow.relay(block, part)
+
+
 def mixer_kernel(
     groups,
     chunk,
@@ -461,8 +566,10 @@
     raw,
     normed,
     w_in,
+    in_stage,
     total,
     w_out,
+    out_stage,
     both,
     acted,
     mixed,
@@ -481,10 +588,10 @@
     start,
     in_sent,
     in_got,
-    in_passed,
+    in_staged,
     out_sent,
     out_got,
-    out_passed,
+    out_staged,
     kept,
     token_sent,
     token_got,
@@ -504,85 +611,139 @@
     side = model // 2
     share = feed.shape[1]
     wide = both.shape[2]
-    token_parts, both_parts = (token_sent.shape[0], both_sent.shape[0])
+    token_parts, both_parts = (token_sent.shape[0], both_sent.shape[0] // 2)
     token_rows, both_rows = (length // token_parts, tokens // both_parts)
 
     def token_view(origin, part, which):
-        rows = span_of(origin * length + part * token_rows, token_rows, 16)
+        rows = span_of((part * 8 + origin) * token_rows, token_rows, 16)
         return normed.at[rows, span_of(which * side, side)]
 
     def both_view(origin, part, which):
         columns = span_of((which * 8 + origin) * share, share)
-        return both.at[:, pl.ds(part * both_rows, both_rows), columns]
+        branch, piece = divmod(part, both_parts)
+        return both.at[branch, pl.ds(piece * both_rows, both_rows), columns]
 
     inward = WeightFlow(
-        place, (value_ref, gate_ref, feed_ref), w_in, in_sent, in_got, in_passed, kept.at[0]
+        place,
+        (value_ref, gate_ref, feed_ref),
+        w_in,
+        in_stage,
+        in_sent,
+        in_got,
+        in_staged,
+        kept.at[0],
     )
     outward = WeightFlow(
-        place, (project_ref, svalue_ref, sgate_ref), w_out, out_sent, out_got, out_passed, kept.at[1]
+        place,
+        (project_ref, svalue_ref, sgate_ref),
+        w_out,
+        out_stage,
+        out_sent,
+        out_got,
+        out_staged,
+        kept.at[1],
     )
     token_flow = GatherFlow(place, token_view, token_parts, token_sent, token_got, 3)
-    both_flow = GatherFlow(place, both_view, both_parts, both_sent, both_got)
-
+    both_flow = GatherFlow(place, both_view, 2 * both_parts, both_sent, both_got)
+
+    barrier = pltpu.get_barrier_semaphore()
+    greeted = [place.lanes["peer"], place.partner]
+    for flip in range(1, 8):
+        for side_of in (half, 1 - half):
+            greeted.append(place.device_of(place.members[flip], side_of))
+    for device in greeted:
+        pl.semaphore_signal(barrier, inc=1, device_id=device, device_id_type=pl.DeviceIdType.MESH)
     load = pltpu.make_async_copy(token_ref, raw, single.at[0])
     load.start()
-    inward.start()
+    inward.hold()
+    outward.hold()
     load.wait()
     gain = gain_ref[...]
+
+    def norm(step, _):
+        floats = raw[span_of(step * 16, 16)].astype(jnp.float32)
+        scale = lax.rsqrt(jnp.mean(floats * floats, axis=1, keepdims=True) + 1e-06)
+        part, within = (step // (token_rows // 16), step % (token_rows // 16))
+        rows = span_of((part * 8 + slot) * token_rows + within * 16, 16)
+        normed[rows] = (floats * scale * gain).astype(jnp.bfloat16)
+        return 0
+
+    lax.fori_loop(0, length // 16, norm, 0)
+    pl.semaphore_wait(barrier, len(greeted))
+    inward.start((1, 2, 3))
+    inward.relay(1, 0)
+    inward.relay(0, 0)
     for part in range(token_parts):
-
-        def norm(step, _):
-            floats = raw[span_of(part * token_rows + step * 16, 16)].astype(jnp.float32)
-            scale = lax.rsqrt(jnp.mean(floats * floats, axis=1, keepdims=True) + 1e-06)
-            rows = span_of(slot * length + part * token_rows + step * 16, 16)
-            normed[rows] = (floats * scale * gain).astype(jnp.bfloat16)
+        token_flow.send(0, part)
+    def build(part):
+        build_matrices(
+            groups, chunk, small_ref, vec_ref, skip_ref, push, emit, inside, span, drive
+        )
+
+    margin = gated.shape[0] - tokens
+    part_rows = 8 * token_rows
+    block_rows = 128
+
+    def gate(part):
+        def apply(step, _):
+            value = total[span_of((part * 8 + step) * token_rows, token_rows, 16)]
+            product = value[:, :share] * jax.nn.sigmoid(value[:, share : 2 * share])
+            begin = step * length + part * token_rows
+            gated[span_of(margin + begin, token_rows, 8)] = product.astype(jnp.bfloat16).astype(
+                jnp.float32
+            )
+            feed[span_of(begin, token_rows, 8)] = (
+                value[:, 2 * share :].astype(jnp.bfloat16).astype(jnp.float32)
+            )
             return 0
 
-        lax.fori_loop(0, token_rows // 16, norm, 0)
-        token_flow.send(0, part)
-    for flip in range(8):
-        inward.relay(flip)
-    build_matrices(
-        groups, chunk, small_ref, vec_ref, skip_ref, push, emit, inside, span, drive
-    )
-    for part in range(token_parts):
-        token_flow.relay(1, part)
-        token_flow.relay(2, part)
-    for part in range(token_parts):
-        token_flow.relay(3, part)
-    outward.start()
-    for part in range(token_parts):
-        for block in range(4, 8):
-            token_flow.relay(block, part)
-    outward.relay(0)
-    for part in range(token_parts):
+        lax.fori_loop(0, 8, apply, 0)
+
+    def arrive(part):
         for block in range(1, 8):
             token_flow.peer_wait(block, part)
 
-    block_rows = 256
-
-    def first_product(step, _):
-        rows = span_of(step * block_rows, block_rows)
-        depth = span_of(half * side, side)
-        total[rows] = dot(normed[rows, depth], w_in[depth])
-        return 0
-
-    lax.fori_loop(0, tokens // block_rows, first_product, 0)
-    depth_size = 2 * inward.rows
-    for flip in range(0, 8, 2):
-        inward.far_wait(flip)
-        inward.far_wait(flip + 1)
-        pair = inward.far_index(flip) // 2
+    def near_product(part):
+        arrive(part)
+        if part == 0:
+            inward.near_wait()
+
+        def first_product(step, _):
+            rows = span_of(part * part_rows + step * block_rows, block_rows)
+            depth = span_of(half * side, side)
+            total[rows] = dot(normed[rows, depth], w_in[depth])
+            return 0
+
+        lax.fori_loop(0, part_rows // block_rows, first_product, 0)
+
+    def far_product(part):
+        if part == 0:
+            for far in range(8):
+                inward.far_wait(far // 4, far % 4)
 
         def add_product(step, _):
-            rows = span_of(step * block_rows, block_rows)
-            depth = span_of(pair * depth_size, depth_size)
+            rows = span_of(part * part_rows + step * block_rows, block_rows)
+            depth = span_of((1 - half) * side, side)
             total[rows] = total[rows] + dot(normed[rows, depth], w_in[depth])
             return 0
 
-        lax.fori_loop(0, tokens // block_rows, add_product, 0)
-
-    margin = gated.shape[0] - tokens
+        lax.fori_loop(0, part_rows // block_rows, add_product, 0)
+        gate(part)
+
+    def whole_product(part):
+        arrive(part)
+
+        def product(step, _):
+            rows = span_of(part * part_rows + step * block_rows, block_rows)
+            total[rows] = dot(normed[rows], w_in[...])
+            return 0
+
+        lax.fori_loop(0, part_rows // block_rows, product, 0)
+        gate(part)
+
+    run_order(
+        ORDER_A, inward, outward, token_flow, (build, near_product, far_product, whole_product)
+    )
     gated_edge = remote(
         gated.at[pl.ds(tokens, margin)],
         gated.at[pl.ds(0, margin)],
@@ -591,18 +752,6 @@
         place.partner,
     )
     state_edge = remote(last, start, edge.at[2], edge.at[3], place.partner)
-
-    def gate(step, _):
-        rows = span_of(step * block_rows, block_rows)
-        value = total[rows]
-        product = value[:, :share] * jax.nn.sigmoid(value[:, share : 2 * share])
-        gated[span_of(margin + step * block_rows, block_rows, 8)] = product.astype(
-            jnp.bfloat16
-        ).astype(jnp.float32)
-        feed[rows] = value[:, 2 * share :].astype(jnp.bfloat16).astype(jnp.float32)
-        return 0
-
-    lax.fori_loop(0, tokens // block_rows, gate, 0)
 
     @pl.when(half == 0)
     def _():
@@ -649,13 +798,20 @@
         scan(vec_ref[2:3], vec_ref[3:4])
         state_edge.start()
 
+    run_order(ORDER_M, inward, outward, None, None)
+
     @pl.when(half == 1)
     def _():
         gated_edge.wait_recv()
 
     own_columns = span_of((core * 8 + slot) * share, share)
     kernel = taps_ref.shape[0]
-    conv_rows = 64
+    conv_rows = token_rows
+    per_member = length // conv_rows
+
+    def shuffled(step):
+        return (step % per_member * 8 + step // per_member) * token_rows
+
     ahead = margin - (kernel - 1)
 
     def convolve(step, _):
@@ -667,10 +823,14 @@
                 if (ahead + tap) % 8 == residue:
                     begin = ahead + tap - residue
                     summed = summed + taps_ref[tap : tap + 1] * shifted[begin : begin + conv_rows]
-        both[0, span_of(step * conv_rows, conv_rows), own_columns] = summed.astype(jnp.bfloat16)
+        rows = span_of(shuffled(step), conv_rows, 16)
+        both[0, rows, own_columns] = summed.astype(jnp.bfloat16)
         return 0
 
     lax.fori_loop(0, tokens // conv_rows, convolve, 0)
+    for part in range(both_parts):
+        both_flow.send(0, part)
+    run_order(ORDER_N, inward, outward, None, None)
 
     def final_copy(slot_to, half_to, number):
         return remote(
@@ -714,69 +874,70 @@
             ]
 
     def store_answer(step, _):
-        rows = span_of(step * block_rows, block_rows)
-        both[1, rows, own_columns] = answer[rows].astype(jnp.bfloat16)
+        value = answer[span_of(step * token_rows, token_rows, 8)]
+        both[1, span_of(shuffled(step), token_rows, 16), own_columns] = value.astype(jnp.bfloat16)
         return 0
 
-    lax.fori_loop(0, tokens // block_rows, store_answer, 0)
+    lax.fori_loop(0, tokens // token_rows, store_answer, 0)
     for part in range(both_parts):
-        both_flow.send(0, part)
+        both_flow.send(0, both_parts + part)
 
     @pl.when(half == 1)
     def _():
         for copy in final_copies():
             copy.start()
 
-    for flip in range(1, 8):
-        outward.relay(flip)
-    for part in range(both_parts):
-        both_flow.relay(1, part)
-        both_flow.relay(2, part)
-    for part in range(both_parts):
-        both_flow.relay(3, part)
-    for flip in range(8):
-        outward.far_wait(flip)
-
     output = w_out.shape[1] // 3
     finish_rows = 128
 
-    def mix_copy(member):
+    def mix_refs(member, part):
+        return (
+            mixed.at[pl.ds((part * 8 + member) * token_rows, token_rows)],
+            out_ref.at[pl.ds(part * token_rows, token_rows), span_of(slot * output, output)],
+        )
+
+    def mix_copy(member, refs):
         return remote(
-            mixed.at[pl.ds(member * length, length)],
-            out_ref.at[:, span_of(slot * output, output)],
-            mix_sent.at[member],
-            mix_got.at[slot],
-            place.device_of(member, half),
+            *refs, mix_sent.at[member], mix_got.at[slot], place.device_of(member, half)
         )
 
-    def mix_keep(member):
-        return pltpu.make_async_copy(
-            mixed.at[pl.ds(member * length, length)],
-            out_ref.at[:, span_of(slot * output, output)],
-            mix_sent.at[member],
-        )
-
-    for part in range(both_parts):
-        for block in range(4, 8):
-            both_flow.relay(block, part)
+    def mix_keep(member, refs):
+        return pltpu.make_async_copy(*refs, mix_sent.at[member])
+
+    chan_gain, chan_shift = (chan_gain_ref[...], chan_shift_ref[...])
+
+    def normalise(part):
         for block in range(8):
             both_flow.peer_wait(block, part)
 
         def activate(step, _):
-            rows = span_of(step * 16, 16)
-            full = both[0, span_of(part * both_rows + step * 16, 16)].astype(jnp.float32)
-            centred = full - jnp.mean(full, axis=1, keepdims=True)
-            variance = jnp.mean(centred * centred, axis=1, keepdims=True)
-            value = centred * lax.rsqrt(variance + 1e-05) * chan_gain_ref[...] + chan_shift_ref[...]
-            acted[rows] = jax.nn.silu(value).astype(jnp.bfloat16)
+            for offset in range(2):
+                rows = span_of(part * both_rows + step * 32 + offset * 16, 16)
+                full = both[0, rows].astype(jnp.float32)
+                centred = full - jnp.mean(full, axis=1, keepdims=True)
+                variance = jnp.mean(centred * centred, axis=1, keepdims=True)
+                value = centred * lax.rsqrt(variance + 1e-05) * chan_gain + chan_shift
+                bent = 0.5 * value
+                acted[rows] = (bent + bent * jnp.tanh(bent)).astype(jnp.bfloat16)
             return 0
 
-        lax.fori_loop(0, both_rows // 16, activate, 0)
+        lax.fori_loop(0, both_rows // 32, activate, 0)
+
+    def settle(part):
+        inward.drain()
+        token_flow.drain()
+
+    def conclude(part):
+        for block in range(8):
+            both_flow.peer_wait(block, both_parts + part)
+        if part == 0:
+            outward.near_wait()
+            for far in range(8):
+                outward.far_wait(far // 4, far % 4)
 
         def finish(step, _):
-            local_rows = span_of(step * finish_rows, finish_rows)
             rows = span_of(part * both_rows + step * finish_rows, finish_rows)
-            branch = dot(acted[local_rows], w_out[:, :output])
+            branch = dot(acted[rows], w_out[:, :output])
             state = dot(both[1, rows], w_out[:, output:])
             mixed[rows] = (
                 branch + state[:, :output] * jax.nn.sigmoid(state[:, output:])
@@ -784,19 +945,13 @@
             return 0
 
         lax.fori_loop(0, both_rows // finish_rows, finish, 0)
-        for member in range(part * both_rows // length, (part + 1) * both_rows // length):
-
-            @pl.when(slot == member)
-            def _():
-                mix_keep(member).start()
-
-            @pl.when(slot != member)
-            def _():
-                mix_copy(member).start()
-
-    inward.drain()
+        for member in range(8):
+            refs = mix_refs(member, part)
+            pl.when(slot == member)(mix_keep(member, refs).start)
+            pl.when(slot != member)(mix_copy(member, refs).start)
+
+    run_order(ORDER_B, inward, outward, both_flow, (normalise, conclude, settle))
     outward.drain()
-    token_flow.drain()
     both_flow.drain()
 
     @pl.when(half == 0)
@@ -821,14 +976,12 @@
             copy.wait_send()
 
     for member in range(8):
-
-        @pl.when(slot == member)
-        def _():
-            mix_keep(member).wait()
-
-        @pl.when(slot != member)
-        def _():
-            mix_copy(member).wait_send()
+        refs = (
+            mixed.at[pl.ds(0, length)],
+            out_ref.at[:, span_of(slot * output, output)],
+        )
+        pl.when(slot == member)(mix_keep(member, refs).wait)
+        pl.when(slot != member)(mix_copy(member, refs).wait_send)
 
     for flip in range(1, 8):
         origin = place.members[flip]
@@ -904,7 +1057,7 @@
     dma = pltpu.SemaphoreType.DMA
     half_word, word = (jnp.bfloat16, jnp.float32)
     margin = 32
-    token_parts, both_parts = (2, 4)
+    token_parts, both_parts = (4, 4)
     count = span // chunk
     any_spec = pl.BlockSpec(memory_space=pl.ANY)
     near_spec = pl.BlockSpec(memory_space=pltpu.VMEM)
@@ -920,10 +1073,12 @@
             vmem((length, model), half_word),
             vmem((span, model), half_word),
             vmem((devices * conv_value.shape[0], 3 * share), half_word),
+            vmem((4, conv_value.shape[0], 3 * share), half_word),
             vmem((span, 3 * share), word),
             vmem((devices * conv_project.shape[0], 3 * output), half_word),
+            vmem((4, conv_project.shape[0], 3 * output), half_word),
             vmem((2, span, wide), half_word),
-            vmem((span // both_parts, wide), half_word),
+            vmem((span, wide), half_word),
             vmem((span, output), half_word),
             vmem((margin + span, share), word),
             vmem((span, share), word),
@@ -938,17 +1093,17 @@
             vmem((2, flat), word),
             vmem((2 * flat // 128, 128), word),
             vmem((2 * flat // 128, 128), word),
-            dma((7,)),
+            dma((6, 4)),
             dma((16,)),
-            dma((8,)),
-            dma((7,)),
+            dma((4,)),
+            dma((6, 4)),
             dma((16,)),
-            dma((8,)),
-            dma((2, 3)),
+            dma((4,)),
+            dma((2, 2, 3)),
             dma((token_parts, 15)),
             dma((8, 2 * token_parts)),
-            dma((both_parts, 15)),
-            dma((8, 2 * both_parts)),
+            dma((2 * both_parts, 15)),
+            dma((8, 4 * both_parts)),
             dma((8,)),
             dma((8,)),
             dma((16,)),
@@ -957,7 +1112,7 @@
             dma((2,)),
         ],
         compiler_params=pltpu.CompilerParams(
-            has_side_effects=True, vmem_limit_bytes=67043328
+            has_side_effects=True, collective_id=0, vmem_limit_bytes=67043328
         ),
     )(
         tokens,

time: 262 us -> 195 us (0.74)
  Pallas kernels: 249 us -> 182 us
    pallas_call x1, Pallas kernels: 249 us -> 182 us  [cube_local(): pl.pallas_call(functools.partial(mixer_kernel, groups, chunk), out_shape=...]
where the time goes in v2:
time: 195 us; the launch traced here: 194 us
  Pallas kernels  182 us (93%)
  local copies, waits for them, and re-layouts  8.43 us (4%)
  other arithmetic  2.91 us (1%)
    pallas_call x1, Pallas kernels, cube_local(): pl.pallas_call(functools.partial(mixer_kernel, groups, chunk), out_shape=...  182 us

profile of v2, /device:TPU:0, one launch (start us, length us, event | category | flops | bytes accessed | tf_op | source)
XLA Modules:
  0.0 194.0 jit_solution(12369103109084618588)
XLA Ops:
  0.7 1.3 dynamic-slice_bitcast_fusion.2.skip_ref
  2.0 0.7 constant_dynamic-slice_fusion.1
  2.7 0.1 stack.14
  2.8 1.3 constant_dynamic-slice_fusion.taps_ref
  4.1 0.7 cosine_multiply_fusion
  4.8 0.1 stack.12
  4.9 0.1 stack.13
  5.0 0.6 pad_maximum_fusion.1.vec_ref
  5.6 0.9 subtract_bitcast_fusion
  6.5 0.1 reshape.30
  6.6 0.1 reshape.31
  6.7 0.9 dynamic-slice_bitcast_fusion
  7.6 0.1 reshape.33
  7.7 0.1 reshape.32
  7.8 0.7 pad_maximum_fusion.small_ref
  8.5 181.9 %shard_map.194 = (bf16[192,2048]{1,0:T(8,128)(2,1)}, f32[8,8,128]{2,1,0:T(8,128)}) custom-call(bf16[192,4096]{1,0:T(8,128)(2,1)} %token_ref.1, bf16[256,1024]{1,0:T(8,128)(2,1)} %value_ref.1, bf16[256,1024]{1,0:T(8,128)(2,1)} %gate_ref.1, bf16[256,1024]{1,0:T(8,128)(2,1)} %feed_ref.1, bf16[128,2048]{1,0:T(8,128)(2,1)} %project_ref.1, ...), custom_call_target="tpu_custom_call" | custom-call | tf_op jit(solution)/shard_map/pallas_call | solution.py:1064
  190.4 0.8 reshape.34
  191.2 0.6 copy_bitcast_fusion
  191.9 2.1 %copy.28 = bf16[192,2048]{1,0:T(8,128)(2,1)} copy(bf16[192,2048]{1,0:T(8,128)(2,1)} %get-tuple-element.16) | data formatting | bytes 1572864
  (4 shorter events, 0.1 us)

commit v3 on v2

--- a/solution.py
+++ b/solution.py
@@ -452,24 +452,45 @@
     return (high, (value - high.astype(jnp.float32)).astype(jnp.bfloat16))
 
 
-def build_matrices(groups, chunk, small_ref, vec_ref, skip_ref, push, emit, inside, span, drive):
-    width = small_ref.shape[0] // 4
-    flat = small_ref.shape[1]
+def in_rows(piece):
+    return jnp.concatenate([piece[group : group + 1] for group in range(piece.shape[0])], axis=1)
+
+
+def build_matrices(
+    total, chunk, rates, inputs, outputs, skip_ref, push, emit, inside, span, drive
+):
+    groups, states = rates.shape[1:]
+    width = inputs.shape[2]
+    flat = groups * states
     lanes = groups * width
     row_group = lax.broadcasted_iota(jnp.int32, (lanes, flat), 0) // width
-    column_group = lax.broadcasted_iota(jnp.int32, (lanes, flat), 1) // (flat // groups)
+    column_group = lax.broadcasted_iota(jnp.int32, (lanes, flat), 1) // states
     mask = (row_group == column_group).astype(jnp.float32)
 
-    def spread(which):
-        return jnp.concatenate([small_ref[which * width : (which + 1) * width]] * groups, 0) * mask
-
-    step_real, step_imag = (vec_ref[0:1], vec_ref[1:2])
+    def spread(value):
+        return jnp.concatenate([value] * groups, 0) * mask
+
+    rate, turn = (in_rows(-rates[0] / total), in_rows(rates[1]))
+    magnitude = jnp.exp(rate)
+    step_real, step_imag = (magnitude * jnp.cos(turn), magnitude * jnp.sin(turn))
+    modulus = rate * rate + turn * turn
+    lift = step_real - 1.0
+    factor_real = (lift * rate + step_imag * turn) / modulus
+    factor_imag = (step_imag * rate - lift * turn) / modulus
+    in_real, in_imag = (
+        jnp.concatenate([inputs[side, group] for group in range(groups)], axis=1)
+        for side in range(2)
+    )
+    out_real, out_imag = (
+        spread(jnp.concatenate([outputs[side, group] for group in range(groups)], axis=1))
+        for side in range(2)
+    )
     powers = [(jnp.ones_like(step_real), jnp.zeros_like(step_real))]
     for _ in range(chunk):
         powers.append(rotate(*powers[-1], step_real, step_imag))
     span[0:1] = powers[chunk][0]
     span[1:2] = powers[chunk][1]
-    drive_real, drive_imag = (spread(0), spread(1))
+    drive_real, drive_imag = map(spread, rotate(factor_real, factor_imag, in_real, in_imag))
     for place in range(chunk):
         rows = pl.ds(place * lanes, lanes)
         for side, value in enumerate(rotate(*powers[chunk - 1 - place], drive_real, drive_imag)):
@@ -478,7 +499,6 @@
     for side, value in enumerate((drive_real, drive_imag)):
         for part, piece in enumerate(halves(value)):
             drive[part, :, pl.ds(side * flat, flat)] = piece
-    out_real, out_imag = (spread(2), spread(3))
     inside[...] = jnp.zeros_like(inside)
     diagonal = lax.broadcasted_iota(jnp.int32, (lanes, lanes), 0) == lax.broadcasted_iota(
         jnp.int32, (lanes, lanes), 1
@@ -510,19 +530,16 @@
 ORDER_A = (
     "i11", "i01", "i12", "i02", "r10", "r20", "i13", "i03", "r11", "r21", "r30", "w00", "i20",
     "r12", "r22", "r31", "r40", "i21", "i22", "r13", "r23", "r32", "r41", "i23", "w10", "r33",
-    "s13", "r42", "w11", "w20", "w21", "w32", "r43", "w33",
+    "s13", "r42", "o10", "o00", "w11", "w20", "w21", "w32", "r43", "w33",
 )
 ORDER_M = (
-    "o10", "o00",
-)
-ORDER_N = (
-    "o11", "o12", "o01",
+    "o11", "o01",
 )
 ORDER_B = (
-    "r10", "r20", "r11", "r21", "o13", "r12", "r22", "o02", "r13", "r23", "o03", "r30", "r31",
-    "r14", "r24", "o20", "r32", "r33", "r15", "r25", "o21", "r16", "r26", "r17", "r27", "o22",
-    "o23", "r40", "w20", "w00", "r34", "r41", "w01", "r35", "r42", "w02", "r36", "r43", "w03",
-    "r37", "r44", "w10", "r45", "w11", "r46", "w12", "r47", "w13",
+    "r10", "r20", "o12", "r11", "r21", "o02", "r12", "r22", "o13", "r13", "r23", "o03", "r30",
+    "r31", "r14", "r24", "o20", "r32", "r33", "r15", "r25", "o21", "r16", "r26", "r17", "r27",
+    "o22", "o23", "r40", "w20", "w00", "r34", "r41", "w01", "r35", "r42", "w02", "r36", "r43",
+    "w03", "r37", "r44", "r45", "r46", "r47", "w10", "w11", "w12", "w13",
 )
 
 
@@ -545,7 +562,6 @@
 
 
 def mixer_kernel(
-    groups,
     chunk,
     token_ref,
     value_ref,
@@ -554,11 +570,16 @@
     project_ref,
     svalue_ref,
     sgate_ref,
+    taps_from,
+    decay_from,
+    turn_from,
+    in_real_from,
+    in_imag_from,
+    out_real_from,
+    out_imag_from,
+    skip_from,
+    state_from,
     gain_ref,
-    small_ref,
-    vec_ref,
-    taps_ref,
-    skip_ref,
     chan_gain_ref,
     chan_shift_ref,
     out_ref,
@@ -603,6 +624,13 @@
     final_got,
     edge,
     single,
+    taps_ref,
+    rates,
+    inputs,
+    outputs,
+    skip_ref,
+    begin,
+    small_sem,
 ):
     place = Place()
     half, slot, core = (place.half, place.slot, place.core)
@@ -655,6 +683,26 @@
         pl.semaphore_signal(barrier, inc=1, device_id=device, device_id_type=pl.DeviceIdType.MESH)
     load = pltpu.make_async_copy(token_ref, raw, single.at[0])
     load.start()
+    own_groups = span_of(slot * rates.shape[1], rates.shape[1])
+    own_lanes = span_of(slot * share, share)
+    small = [
+        pltpu.make_async_copy(origin, target, small_sem.at[number])
+        for number, (origin, target) in enumerate(
+            (
+                (taps_from.at[:, own_lanes], taps_ref),
+                (decay_from.at[own_groups], rates.at[0]),
+                (turn_from.at[own_groups], rates.at[1]),
+                (in_real_from.at[own_groups], inputs.at[0]),
+                (in_imag_from.at[own_groups], inputs.at[1]),
+                (out_real_from.at[own_groups], outputs.at[0]),
+                (out_imag_from.at[own_groups], outputs.at[1]),
+                (skip_from.at[:, own_lanes], skip_ref),
+                (state_from.at[:, own_groups], begin),
+            )
+        )
+    ]
+    for copy in small:
+        copy.start()
     inward.hold()
     outward.hold()
     load.wait()
@@ -676,8 +724,10 @@
     for part in range(token_parts):
         token_flow.send(0, part)
     def build(part):
+        for copy in small:
+            copy.wait()
         build_matrices(
-            groups, chunk, small_ref, vec_ref, skip_ref, push, emit, inside, span, drive
+            2 * tokens, chunk, rates, inputs, outputs, skip_ref, push, emit, inside, span, drive
         )
 
     margin = gated.shape[0] - tokens
@@ -789,13 +839,15 @@
             return (real, imag)
 
         real, imag = lax.fori_loop(0, count // 8, advance, (real, imag))
-        for row in range(flat // 128):
-            last[row : row + 1] = real[:, row * 128 : (row + 1) * 128]
-            last[flat // 128 + row : flat // 128 + row + 1] = imag[:, row * 128 : (row + 1) * 128]
+        states = last.shape[2]
+        for group in range(last.shape[1]):
+            columns = slice(group * states, (group + 1) * states)
+            last[0, group : group + 1] = real[:, columns]
+            last[1, group : group + 1] = imag[:, columns]
 
     @pl.when(half == 0)
     def _():
-        scan(vec_ref[2:3], vec_ref[3:4])
+        scan(in_rows(begin[0]), in_rows(begin[1]))
         state_edge.start()
 
     run_order(ORDER_M, inward, outward, None, None)
@@ -830,18 +882,17 @@
     lax.fori_loop(0, tokens // conv_rows, convolve, 0)
     for part in range(both_parts):
         both_flow.send(0, part)
-    run_order(ORDER_N, inward, outward, None, None)
 
     def final_copy(slot_to, half_to, number):
         return remote(
             last,
-            final_ref.at[slot],
+            final_ref.at[:, own_groups],
             final_sent.at[number],
             final_got.at[slot],
             place.device_of(slot_to, half_to),
         )
 
-    final_keep = pltpu.make_async_copy(last, final_ref.at[slot], single.at[1])
+    final_keep = pltpu.make_async_copy(last, final_ref.at[:, own_groups], single.at[1])
 
     def final_copies():
         for flip in range(1, 8):
@@ -852,11 +903,7 @@
     @pl.when(half == 1)
     def _():
         state_edge.wait_recv()
-        rows = flat // 128
-        scan(
-            jnp.concatenate([start[row : row + 1] for row in range(rows)], axis=1),
-            jnp.concatenate([start[rows + row : rows + row + 1] for row in range(rows)], axis=1),
-        )
+        scan(in_rows(start[0]), in_rows(start[1]))
         final_keep.start()
 
     for pair in range(chunk // 2):
@@ -962,7 +1009,11 @@
     for flip in range(8):
         origin = place.members[flip]
         arrival = remote(
-            last, final_ref.at[origin], final_sent.at[0], final_got.at[origin], place.partner
+            last,
+            final_ref.at[:, span_of(origin * last.shape[1], last.shape[1])],
+            final_sent.at[0],
+            final_got.at[origin],
+            place.partner,
         )
         if flip == 0:
             pl.when(half == 0)(arrival.wait_recv)
@@ -1017,7 +1068,6 @@
 ):
     outer, inner = (lax.axis_size("outer"), lax.axis_size("inner"))
     devices = outer * inner
-    slot = lax.axis_index("outer") % 2 * inner + lax.axis_index("inner")
     length, model = tokens.shape
     span = length * devices // 2
     wide = chan_gain.shape[0]
@@ -1028,31 +1078,6 @@
     flat = groups * states
     chunk = 8
 
-    def own(value, size, axis=0):
-        return lax.dynamic_slice_in_dim(value, slot * size, size, axis=axis)
-
-    rate_real = -own(decay_rate, groups) / (length * devices)
-    turn = own(frequency, groups)
-    magnitude = jnp.exp(rate_real)
-    step_real = magnitude * jnp.cos(turn)
-    step_imag = magnitude * jnp.sin(turn)
-    modulus = rate_real * rate_real + turn * turn
-    lift_real = step_real - 1.0
-    factor_real = (lift_real * rate_real + step_imag * turn) / modulus
-    factor_imag = (step_imag * rate_real - lift_real * turn) / modulus
-    in_real, in_imag = (own(input_real, groups), own(input_imag, groups))
-    drive_real = factor_real[..., None] * in_real - factor_imag[..., None] * in_imag
-    drive_imag = factor_real[..., None] * in_imag + factor_imag[..., None] * in_real
-    small = jnp.concatenate(
-        [value.transpose(2, 0, 1).reshape(width, flat) for value in (drive_real, drive_imag)]
-        + [
-            own(value, groups).transpose(1, 0, 2).reshape(width, flat)
-            for value in (output_real, output_imag)
-        ],
-        axis=0,
-    )
-    begin = own(initial_state, groups, 1)
-    vec = jnp.stack([step_real, step_imag, begin[0], begin[1]]).reshape(4, flat)
     vmem = functools.partial(pltpu.VMEM)
     dma = pltpu.SemaphoreType.DMA
     half_word, word = (jnp.bfloat16, jnp.float32)
@@ -1061,13 +1086,13 @@
     count = span // chunk
     any_spec = pl.BlockSpec(memory_space=pl.ANY)
     near_spec = pl.BlockSpec(memory_space=pltpu.VMEM)
-    mixer_out, final = pl.pallas_call(
-        functools.partial(mixer_kernel, groups, chunk),
+    return pl.pallas_call(
+        functools.partial(mixer_kernel, chunk),
         out_shape=(
             jax.ShapeDtypeStruct((length, 8 * output), half_word),
-            jax.ShapeDtypeStruct((8, 2 * flat // 128, 128), word),
+            jax.ShapeDtypeStruct(initial_state.shape, word),
         ),
-        in_specs=[any_spec] * 7 + [near_spec] * 7,
+        in_specs=[any_spec] * 16 + [near_spec] * 3,
         out_specs=(any_spec, any_spec),
         scratch_shapes=[
             vmem((length, model), half_word),
@@ -1091,8 +1116,8 @@
             vmem((2, chunk * share, chunk * share), half_word),
             vmem((2, share, 2 * flat), half_word),
             vmem((2, flat), word),
-            vmem((2 * flat // 128, 128), word),
-            vmem((2 * flat // 128, 128), word),
+            vmem((2, groups, states), word),
+            vmem((2, groups, states), word),
             dma((6, 4)),
             dma((16,)),
             dma((4,)),
@@ -1110,6 +1135,13 @@
             dma((8,)),
             dma((4,)),
             dma((2,)),
+            vmem((conv_taps.shape[0], share), word),
+            vmem((2, groups, states), word),
+            vmem((2, groups, width, states), word),
+            vmem((2, groups, width, states), word),
+            vmem((1, share), word),
+            vmem((2, groups, states), word),
+            dma((9,)),
         ],
         compiler_params=pltpu.CompilerParams(
             has_side_effects=True, collective_id=0, vmem_limit_bytes=67043328
@@ -1122,16 +1154,19 @@
         conv_project,
         state_value,
         state_gate,
+        conv_taps,
+        decay_rate,
+        frequency,
+        input_real.transpose(0, 2, 1),
+        input_imag.transpose(0, 2, 1),
+        output_real,
+        output_imag,
+        skip_gain[None],
+        initial_state,
         norm_gain[None],
-        small,
-        vec,
-        own(conv_taps, share, 1),
-        own(skip_gain, share)[None],
         chan_gain[None],
         chan_shift[None],
     )
-    final_state = final.reshape(8, 2, groups, states).transpose(1, 0, 2, 3)
-    return (mixer_out, final_state.reshape(2, 8 * groups, states))
 
 
 def specs_of(seq):

time: 195 us -> 175 us (0.90)
  Pallas kernels: 182 us -> 172 us
  local copies, waits for them, and re-layouts: 8.43 us -> 2.75 us
  other arithmetic: 2.91 us -> 0 us
    pallas_call x1, Pallas kernels: 182 us -> 172 us  [cube_local(): pl.pallas_call(functools.partial(mixer_kernel, chunk), out_shape=(jax.Sha...]
    dynamic_slice x2 -> x0, local copies, waits for them, and re-layouts: 2.02 us -> none  [own(): return lax.dynamic_slice_in_dim(value, slot * size, size, axis=axis)]
where the time goes in v3:
time: 175 us
  Pallas kernels  172 us (98%)
  local copies, waits for them, and re-layouts  2.75 us (2%)
    pallas_call x1, Pallas kernels, cube_local(): pl.pallas_call(functools.partial(mixer_kernel, chunk), out_shape=(jax.Sha...  172 us

profile of v3, /device:TPU:0, one launch (start us, length us, event | category | flops | bytes accessed | tf_op | source)
XLA Modules:
  0.0 175.0 jit_solution(12312965281963961066)
XLA Ops:
  0.6 171.6 %shard_map.194 = (bf16[192,2048]{1,0:T(8,128)(2,1)}, f32[2,64,64]{2,1,0:T(8,128)}) custom-call(bf16[192,4096]{1,0:T(8,128)(2,1)} %token_ref.1, bf16[256,1024]{1,0:T(8,128)(2,1)} %value_ref.1, bf16[256,1024]{1,0:T(8,128)(2,1)} %gate_ref.1, bf16[256,1024]{1,0:T(8,128)(2,1)} %feed_ref.1, bf16[128,2048]{1,0:T(8,128)(2,1)} %project_ref.1, ...), custom_call_target="tpu_custom_call" | custom-call | tf_op jit(solution)/shard_map/pallas_call | solution.py:1089
  172.3 0.0 copy-start
  172.3 2.1 %copy.23 = bf16[192,2048]{1,0:T(8,128)(2,1)} copy(bf16[192,2048]{1,0:T(8,128)(2,1)} %get-tuple-element.4) | data formatting | bytes 1572864
  174.4 0.0 copy-done
  174.4 0.6 copy.24
Async XLA Ops:
  172.3 2.1 %copy-start = (f32[2,64,64]{2,1,0:T(8,128)S(1)}, f32[2,64,64]{2,1,0:T(8,128)}, u32[]{:S(2)}) copy-start(f32[2,64,64]{2,1,0:T(8,128)} %get-tuple-element.5) | copy-start | bytes 98308

commit v4 on v3

--- a/solution.py
+++ b/solution.py
@@ -538,8 +538,8 @@
 ORDER_B = (
     "r10", "r20", "o12", "r11", "r21", "o02", "r12", "r22", "o13", "r13", "r23", "o03", "r30",
     "r31", "r14", "r24", "o20", "r32", "r33", "r15", "r25", "o21", "r16", "r26", "r17", "r27",
-    "o22", "o23", "r40", "w20", "w00", "r34", "r41", "w01", "r35", "r42", "w02", "r36", "r43",
-    "w03", "r37", "r44", "r45", "r46", "r47", "w10", "w11", "w12", "w13",
+    "o22", "o23", "r40", "w20", "r34", "r41", "r35", "w00", "r42", "r36", "w01", "r43", "r37",
+    "w02", "r44", "r45", "w03", "r46", "w10", "r47", "w11", "w12", "w13",
 )
 
 

time: 175 us -> 172 us (0.983)
  Pallas kernels: 172 us -> 169 us
    pallas_call x1, Pallas kernels: 172 us -> 169 us  [cube_local(): pl.pallas_call(functools.partial(mixer_kernel, chunk), out_shape=(jax.Sha...]
where the time goes in v4:
time: 172 us
  Pallas kernels  169 us (98%)
  local copies, waits for them, and re-layouts  2.75 us (2%)
    pallas_call x1, Pallas kernels, cube_local(): pl.pallas_call(functools.partial(mixer_kernel, chunk), out_shape=(jax.Sha...  169 us

profile of v4, /device:TPU:0, one launch (start us, length us, event | category | flops | bytes accessed | tf_op | source)
XLA Modules:
  0.0 171.9 jit_solution(7671082839186096515)
XLA Ops:
  0.6 168.5 %shard_map.194 = (bf16[192,2048]{1,0:T(8,128)(2,1)}, f32[2,64,64]{2,1,0:T(8,128)}) custom-call(bf16[192,4096]{1,0:T(8,128)(2,1)} %token_ref.1, bf16[256,1024]{1,0:T(8,128)(2,1)} %value_ref.1, bf16[256,1024]{1,0:T(8,128)(2,1)} %gate_ref.1, bf16[256,1024]{1,0:T(8,128)(2,1)} %feed_ref.1, bf16[128,2048]{1,0:T(8,128)(2,1)} %project_ref.1, ...), custom_call_target="tpu_custom_call" | custom-call | tf_op jit(solution)/shard_map/pallas_call | solution.py:1089
  169.2 0.0 copy-start
  169.2 2.1 %copy.23 = bf16[192,2048]{1,0:T(8,128)(2,1)} copy(bf16[192,2048]{1,0:T(8,128)(2,1)} %get-tuple-element.4) | data formatting | bytes 1572864
  171.3 0.0 copy-done
  171.3 0.6 copy.24
Async XLA Ops:
  169.2 2.1 %copy-start = (f32[2,64,64]{2,1,0:T(8,128)S(1)}, f32[2,64,64]{2,1,0:T(8,128)}, u32[]{:S(2)}) copy-start(f32[2,64,64]{2,1,0:T(8,128)} %get-tuple-element.5) | copy-start | bytes 98308
